TPU v7x, 128 devices: a whole 4x4x4 slice. The times are simulated.
128 devices in a mesh: ep: 64 (over z, y, x), tp: 2 (over core).
Axes of the slice: x: 4, y: 4, z: 4, core: 2. Of those that a mesh axis runs over, the one named last changes fastest.
Arguments:
- tokens: bfloat16 [2048, 3072], P('ep'), may hold values from -6 to 6
- carried: float32 [2048, 96, 128], P('ep', 'tp'), may hold values from -4 to 4
- decay_rate: float32 [96, 64], P('tp'), may hold values from 0.02 to 20
- frequency: float32 [96, 64], P('tp'), may hold values from 0 to 200
- log_step: float32 [96], P('tp'), may hold values from -4.6 to 0
- in_map: bfloat16 [96, 128, 16], P('tp'), may hold values from -1 to 1
- out_map: bfloat16 [96, 16, 128], P('tp'), may hold values from -0.5 to 0.5
- skip_gain: float32 [1536], P('tp'), may hold values from -4 to 4
- norm_gain: float32 [3072], replicated, may hold values from 0.1 to 1.9
- w_in: bfloat16 [3072, 1536], P(None, 'tp'), may hold values from -0.109375 to 0.109375
- w_out: bfloat16 [1536, 3072], P('tp'), may hold values from -0.15625 to 0.15625
- expert_gain: float32 [3072], replicated, may hold values from 0.1 to 1.9
- route_ids: int32 [2048, 2], P('ep'), may hold values from 0 to 7, all different within a row; in each aligned block of 32 rows (0 to 31, 32 to 63, ...) at most 16 rows name the same one
- route_logit: float32 [2048, 2], P('ep'), may hold values from -6 to 6
- w_gate: bfloat16 [3072, 43008], P(None, ('ep', 'tp')), may hold values from -0.109375 to 0.109375
- w_up: bfloat16 [3072, 43008], P(None, ('ep', 'tp')), may hold values from -0.109375 to 0.109375
- w_down: bfloat16 [43008, 3072], P(('ep', 'tp')), may hold values from -0.078125 to 0.078125
Outputs:
- new_tokens: bfloat16 [2048, 3072], P('ep', 'tp')
- new_carried: float32 [2048, 96, 128], P('ep', 'tp')
Inputs may be any that keep to these rules, and one draw needn't show every extreme that they name: `route_ids`: each row names 2 different experts; within each aligned block of 32 rows (the rows of one index of ep) no expert is named by more than 16 rows, a bound that some block reaches.
All inputs are finite; a program needn't handle non-finite values.
Results may differ from a plain program's by a relative error of at most 0.014.
Values may be sent and summed in bfloat16 or wider, within the bound.
No kernel may reach another device: no remote copies, remote signals or barrier semaphores. Data moves between devices by JAX's collectives and lax.ppermute only.
A program may use at most 128 MiB of HBM per device.

v0:
```python
import jax
import jax.numpy as jnp
from jax import lax
from jax.experimental import pallas as pl
from jax.experimental.layout import Layout, with_layout_constraint
from jax.experimental.pallas import tpu as pltpu
from jax.sharding import PartitionSpec as P

EXPERTS = 8
TOP = 2
CAP = 16
Y_SIZE = 4
X_SIZE = 4
SELECT = ("za", "zb", "yb")
SPREAD = ("ya", "xa", "xb")
COLOURS = ((0, 3), (3, 6), (6, 8))
UNIT_CHUNK = 256
OUT_CHUNK = 512
COPY_GROUPS = 2


def gray(value):
    return value ^ (value >> 1)


def neighbour(chip, link):
    place = {"z": chip // (Y_SIZE * X_SIZE), "y": chip // X_SIZE % Y_SIZE, "x": chip % X_SIZE}
    axis, bit = link
    code = gray(place[axis]) ^ (1 if bit == "a" else 2)
    place[axis] = code ^ (code >> 1)
    return (place["z"] * Y_SIZE + place["y"]) * X_SIZE + place["x"]


def over_links(shard, links):
    pairs = []
    for chip in range(lax.axis_size("ep")):
        other = chip
        for link in links:
            other = neighbour(other, link)
        pairs += [(chip * 2 + core, other * 2 + core) for core in range(2)]
    return lax.ppermute(shard, ("ep", "tp"), pairs)


def select_links(block):
    return [link for bit, link in zip((4, 2, 1), SELECT) if block & bit]


def spread_links(step, colour):
    return [SPREAD[(step + colour) % 3]]


def swapped(shard):
    return lax.ppermute(shard, "tp", [(0, 1), (1, 0)])


def load_kernel(units, *refs):
    sources, helds, sem = refs[0:6], refs[-4:-1], refs[-1]
    copies = [
        pltpu.make_async_copy(
            source, helds[index // 2].at[pl.ds(index % 2 * units, units)], sem.at[index]
        )
        for index, source in enumerate(sources)
    ]
    for copy in copies:
        copy.start()
    for copy in copies:
        copy.wait()


def loaded(gates, ups, downs, after):
    units, width = gates[0].shape
    whole = pl.BlockSpec(memory_space=pl.ANY)
    return pl.pallas_call(
        lambda *refs: load_kernel(units, *refs),
        out_shape=[pltpu.VMEM((2 * units, width), jnp.bfloat16)] * 3,
        in_specs=[whole] * (6 + len(after)),
        out_specs=[pl.BlockSpec(memory_space=pltpu.VMEM)] * 3,
        scratch_shapes=[pltpu.SemaphoreType.DMA((6,))],
        compiler_params=pltpu.CompilerParams(vmem_limit_bytes=2 * 1024 * 1024),
        cost_estimate=pl.CostEstimate(
            flops=6 * units * width * 2048,
            transcendentals=0,
            bytes_accessed=12 * units * width,
        ),
        name="load",
    )(*gates, *ups, *downs, *after)


def expert_kernel(sizes, targets, *refs):
    count = len(sizes)
    pieces, (gate, up, down) = refs[:count], refs[count : count + 3]
    out, rows, hidden, result, out_sem = refs[-5:]
    for index, piece in enumerate(pieces):
        rows[pl.ds(sum(sizes[:index]), sizes[index]), :] = piece[...]
    contract = (((1,), (1,)), ((), ()))
    units = gate.shape[0]
    for first in range(0, units, UNIT_CHUNK):
        span = pl.ds(first, min(UNIT_CHUNK, units - first))
        gated = lax.dot_general(
            rows[...], gate[span, :], contract, preferred_element_type=jnp.float32
        )
        upward = lax.dot_general(
            rows[...], up[span, :], contract, preferred_element_type=jnp.float32
        )
        hidden[:, span] = (jax.nn.silu(gated) * upward).astype(hidden.dtype)
    slots, width = out.shape[1:]
    out_copies = []
    for first in range(0, width, OUT_CHUNK):
        span = pl.ds(first, OUT_CHUNK)
        result[:, span] = jnp.dot(
            hidden[...], down[:, span], preferred_element_type=jnp.float32
        ).astype(result.dtype)
        done = first + OUT_CHUNK
        if done % (width // COPY_GROUPS):
            continue
        group = done * COPY_GROUPS // width - 1
        columns = pl.ds(group * (width // COPY_GROUPS), width // COPY_GROUPS)
        for block in range(sum(sizes) // slots):
            copy = pltpu.make_async_copy(
                result.at[pl.ds(block * slots, slots), columns],
                out.at[targets[block], :, columns],
                out_sem.at[group, block],
            )
            copy.start()
            out_copies.append(copy)
    for copy in out_copies:
        copy.wait()


def experts(pieces, targets, held, slots, earlier=()):
    sizes = [piece.shape[0] for piece in pieces]
    units, width = held[0].shape
    count_rows = sum(sizes)
    whole = pl.BlockSpec(memory_space=pl.ANY)
    vmem = pl.BlockSpec(memory_space=pltpu.VMEM)
    first = 1 + len(pieces) + len(held)
    return pl.pallas_call(
        lambda targets, *refs: expert_kernel(sizes, targets, *refs),
        out_shape=jax.ShapeDtypeStruct((lax.axis_size("ep"), slots, width), jnp.bfloat16),
        in_specs=[pl.BlockSpec(memory_space=pltpu.SMEM)]
        + [vmem] * (len(pieces) + len(held))
        + [whole] * len(earlier),
        out_specs=whole,
        input_output_aliases={first: 0} if earlier else {},
        scratch_shapes=[
            pltpu.VMEM((count_rows, width), jnp.bfloat16),
            pltpu.VMEM((count_rows, units), jnp.bfloat16),
            pltpu.VMEM((count_rows, width), jnp.bfloat16),
            pltpu.SemaphoreType.DMA((COPY_GROUPS, count_rows // slots)),
        ],
        compiler_params=pltpu.CompilerParams(vmem_limit_bytes=16 * 1024 * 1024),
        cost_estimate=pl.CostEstimate(
            flops=6 * count_rows * units * width,
            transcendentals=count_rows * units,
            bytes_accessed=4 * count_rows * width,
        ),
        name="experts",
    )(targets, *pieces, *held, *earlier)


def link_mask(links):
    place = {"z": 16, "y": 4, "x": 1}
    return sum(place[link[0]] * (1 if link[1] == "a" else 2) for link in links)


def block_targets():
    masks = []
    for steps in (range(4), range(4, 8)):
        for colour, (first, last) in enumerate(COLOURS):
            for crossed in steps:
                spread = [spread_links(bit, colour)[0] for bit in range(3) if crossed >> bit & 1]
                masks += [link_mask(spread + select_links(block)) for block in range(first, last)]
    chip = lax.axis_index("ep")
    own = gray(chip // 16) * 16 + gray(chip // 4 % 4) * 4 + gray(chip % 4)
    code = own ^ jnp.array(masks, jnp.int32)
    return code ^ (code >> 1 & 21)


def normalize(rows, gain):
    wide = rows.astype(jnp.float32)
    scaled = wide * lax.rsqrt(jnp.mean(wide * wide, axis=-1, keepdims=True) + 1e-06)
    return (scaled * gain).astype(jnp.bfloat16)


def state_update(drive, carried, decay_rate, frequency, log_step, in_map, out_map, skip_gain):
    count_rows, width = drive.shape
    groups, half = decay_rate.shape
    channels = width // groups
    step_size = jnp.exp(log_step)[:, None]
    magnitude = jnp.exp(-decay_rate * step_size)
    real_decay = magnitude * jnp.cos(frequency * step_size)
    imag_decay = magnitude * jnp.sin(frequency * step_size)
    denom = decay_rate * decay_rate + frequency * frequency
    real_less = real_decay - 1.0
    real_factor = (-real_less * decay_rate + imag_decay * frequency) / denom
    imag_factor = (-imag_decay * decay_rate - real_less * frequency) / denom
    grouped_drive = drive.reshape(count_rows, groups, channels)
    projected = jnp.einsum(
        "sgh,gqh->sgq", grouped_drive, in_map, preferred_element_type=jnp.float32
    )
    real_in = projected[..., :half]
    imag_in = projected[..., half:]
    real_push = real_factor * real_in - imag_factor * imag_in
    imag_push = real_factor * imag_in + imag_factor * real_in
    real_old = carried[..., :half]
    imag_old = carried[..., half:]
    real_new = real_decay * real_old - imag_decay * imag_old + real_push
    imag_new = real_decay * imag_old + imag_decay * real_old + imag_push
    joined = jnp.concatenate([real_new, -imag_new], axis=-1)
    reading = jnp.einsum("sgq,ghq->sgh", joined, out_map.astype(jnp.float32))
    total = reading.reshape(count_rows, width) + skip_gain * drive.astype(jnp.float32)
    activated = jax.nn.gelu(total).astype(jnp.bfloat16)
    return (activated, jnp.concatenate([real_new, imag_new], axis=-1))


def route_weights(route_logit):
    first = jax.nn.sigmoid(route_logit[:, 0] - route_logit[:, 1])
    second = jax.nn.sigmoid(route_logit[:, 1] - route_logit[:, 0])
    return jnp.stack([first, second], axis=1)


def per_device(
    tokens,
    carried,
    decay_rate,
    frequency,
    log_step,
    in_map,
    out_map,
    skip_gain,
    norm_gain,
    w_in,
    w_out,
    expert_gain,
    route_ids,
    route_logit,
    w_gate,
    w_up,
    w_down,
):
    count_rows, model_width = tokens.shape
    core = lax.axis_index("tp")
    slots = CAP // lax.axis_size("tp")
    normed = normalize(tokens, norm_gain)
    drive = jnp.dot(normed, w_in, preferred_element_type=jnp.float32).astype(jnp.bfloat16)
    activated, new_carried = state_update(
        drive, carried, decay_rate, frequency, log_step, in_map, out_map, skip_gain
    )
    partial_value = jnp.dot(activated, w_out, preferred_element_type=jnp.float32).astype(
        jnp.bfloat16
    )
    summed = partial_value.astype(jnp.float32) + swapped(partial_value).astype(jnp.float32)
    mixed = (tokens.astype(jnp.float32) + summed).astype(jnp.bfloat16)
    expert_in = normalize(mixed, expert_gain)
    weights = route_weights(route_logit)
    gates = (w_gate.T, swapped(w_gate.T))
    ups = (w_up.T, swapped(w_up.T))
    downs = (w_down, swapped(w_down))
    chip = lax.axis_index("ep")
    own_z, own_y = chip // (Y_SIZE * X_SIZE), chip // X_SIZE % Y_SIZE
    expert_ids = jnp.arange(EXPERTS, dtype=jnp.int32)
    differ_z, differ_y = gray(expert_ids // 2) ^ gray(own_z), expert_ids % 2 ^ (own_y >> 1)
    block_of = (differ_z & 1) * 4 + (differ_z >> 1) * 2 + differ_y
    routes_flat = route_ids.reshape(-1)
    weights_flat = weights.reshape(-1)
    onehot = (routes_flat[:, None] == expert_ids[None, :]).astype(jnp.int32)
    earlier = jnp.cumsum(onehot, axis=0) - onehot
    slot_index = jnp.sum(earlier * onehot, axis=1) - core * slots
    block = jnp.sum(block_of[None, :] * onehot, axis=1)
    held = (slot_index >= 0) & (slot_index < slots)
    row_ids = jnp.arange(EXPERTS * slots, dtype=jnp.int32)[:, None]
    sent_to = jnp.where(held, block * slots + slot_index, -1)
    position = jnp.where(held, routes_flat * slots + slot_index, -1)
    sending = (row_ids == sent_to[None, :]).astype(jnp.float32)
    placement = (row_ids == position[None, :]).astype(jnp.float32)
    per_token = sending.reshape(EXPERTS * slots, count_rows, TOP).sum(axis=2)
    packed = jnp.dot(per_token.astype(jnp.bfloat16), expert_in, preferred_element_type=jnp.float32)
    blocks = packed.astype(jnp.bfloat16).reshape(EXPERTS, slots, model_width)
    came = [blocks[0]] + [
        over_links(blocks[index], select_links(index)) for index in range(1, EXPERTS)
    ]
    near = []
    for colour, (first, last) in enumerate(COLOURS):
        rows = jnp.concatenate(came[first:last], axis=0)
        for step in range(2):
            across = over_links(rows, spread_links(step, colour))
            rows = jnp.concatenate([rows, across], axis=0)
        near.append(rows)
    held_units = loaded(gates, ups, downs, near[-1:])
    far = []
    for colour, rows in enumerate(near):
        far.append(over_links(rows, spread_links(2, colour)))
    targets = block_targets()
    half = targets.shape[0] // 2
    produced = experts(near, targets[:half], held_units, slots)
    produced = experts(far, targets[half:], held_units, slots, (produced,))
    produced, weights_flat, placement = lax.optimization_barrier(
        (produced, weights_flat, placement)
    )
    returned = lax.all_to_all(produced, "ep", split_axis=0, concat_axis=0, tiled=True)
    new_carried = with_layout_constraint(new_carried, Layout(major_to_minor=(0, 1, 2)))
    returned, new_carried = lax.optimization_barrier((returned, new_carried))
    per_expert = returned.reshape(EXPERTS, -1, slots, model_width).astype(jnp.float32).sum(axis=1)
    per_expert = per_expert.reshape(EXPERTS * slots, model_width)
    weighing = (
        (placement * weights_flat[None, :]).reshape(EXPERTS * slots, count_rows, TOP).sum(axis=2)
    )
    expert_sum = jnp.dot(weighing.T, per_expert, preferred_element_type=jnp.float32)
    half_width = model_width // lax.axis_size("tp")
    own_sum = lax.dynamic_slice_in_dim(expert_sum, core * half_width, half_width, 1)
    other_sum = lax.dynamic_slice_in_dim(expert_sum, (1 - core) * half_width, half_width, 1)
    own_mixed = lax.dynamic_slice_in_dim(mixed, core * half_width, half_width, 1)
    new_tokens = (own_mixed.astype(jnp.float32) + (own_sum + swapped(other_sum))).astype(
        jnp.bfloat16
    )
    return (new_tokens, new_carried)


def solution(mesh):
    return jax.shard_map(
        per_device,
        mesh=mesh,
        in_specs=(
            P("ep", None),
            P("ep", "tp", None),
            P("tp", None),
            P("tp", None),
            P("tp"),
            P("tp", None, None),
            P("tp", None, None),
            P("tp"),
            P(),
            P(None, "tp"),
            P("tp", None),
            P(),
            P("ep", None),
            P("ep", None),
            P(None, ("ep", "tp")),
            P(None, ("ep", "tp")),
            P(("ep", "tp"), None),
        ),
        out_specs=(P("ep", "tp"), P("ep", "tp", None)),
        check_vma=False,
    )
```

profile of v0, /device:TPU:0, one launch (start us, length us, event | category | flops | bytes accessed | tf_op | source)
XLA Modules:
  0.0 128.8 jit_solution(4484831658232649669)
XLA Ops:
  0.7 0.7 exp.14
  1.4 1.1 fusion.7
  2.5 3.4 %convolution_convert_fusion.2 = bf16[32,768]{1,0:T(8,128)(2,1)S(1)} fusion(bf16[3072,768]{1,0:T(8,128)(2,1)} %param.27, bf16[32,3072]{1,0:T(8,128)(2,1)} %param.18, f32[3072]{0:T(1024)} %param.26, f32[32]{0:T(128)S(1)} %add_rsqrt_fusion.1), kind=kOutput, calls=%fused_computation.3 | convolution fusion | flops 151412736 | bytes 4976768 | tf_op jit(solution)/shard_map/dot_general | solution.py:245
  6.1 0.3 fusion.47
  6.5 0.5 copy.49
  7.2 1.4 %fusion.44 = (bf16[32,48,64]{2,1,0:T(8,128)(2,1)S(1)}, f32[32,48,64]{2,1,0:T(8,128)}) fusion(f32[32,48,128]{2,1,0:T(8,128)S(1)} %bitcast.25, f32[48,64]{1,0:T(8,128)S(1)} %get-tuple-element.35, f32[48,64]{1,0:T(8,128)S(1)} %get-tuple-element.36, f32[32,48,128]{2,1,0:T(8,128)S(1)} %copy-done.2, f32[48,64]{1,0:T(8,128)S(1)} %get-tuple-element.34, ...), kind=kLoop, calls=%fused_computation.105 | loop fusion | flops 884736 | bytes 2211840 | tf_op jit(solution)/shard_map/neg | solution.py:209
  8.6 1.4 %subtract_add_fusion = f32[32,48,64]{2,1,0:T(8,128)} fusion(f32[32,48,128]{2,1,0:T(8,128)S(1)} %bitcast.26, f32[32,48,128]{2,1,0:T(8,128)S(1)} %copy-done.2, f32[48,64]{1,0:T(8,128)S(1)} %get-tuple-element.35, f32[48,64]{1,0:T(8,128)S(1)} %get-tuple-element.36, f32[48,64]{1,0:T(8,128)S(1)} %get-tuple-element.34, f32[48,64]{1,0:T(8,128)S(1)} %get-tuple-element.33), kind=kLoop, calls=%fused_computation.12 | loop fusion | flops 688128 | bytes 2015232 | tf_op jit(solution)/shard_map/add | solution.py:207
  10.0 1.5 %pad_maximum_fusion = bf16[32,48,128]{2,1,0:T(8,128)(2,1)S(1)} fusion(bf16[32,48,64]{2,1,0:T(8,128)(2,1)S(1)} %get-tuple-element.22, f32[32,48,64]{2,1,0:T(8,128)} %subtract_add_fusion), kind=kLoop, calls=%fused_computation.4 | loop fusion | flops 786432 | bytes 983040 | tf_op jit(solution)/shard_map/concatenate | solution.py:209
  11.5 0.3 fusion.2
  11.9 3.2 %convolution_convert_fusion.1 = bf16[32,3072]{1,0:T(8,128)(2,1)S(1)} fusion(bf16[768,3072]{1,0:T(8,128)(2,1)} %param.28, f32[32,768]{1,0:T(8,128)S(1)} %copy.42, bf16[32,768]{1,0:T(8,128)(2,1)S(1)} %convolution_convert_fusion.2, f32[768]{0:T(1024)S(1)} %copy-done.9), kind=kOutput, calls=%fused_computation.2 | convolution fusion | flops 151388160 | bytes 5065728 | tf_op jit(solution)/shard_map/dot_general | solution.py:249
  15.2 0.5 collective-permute-start.17
  15.8 0.4 collective-permute-start.19
  17.1 0.7 fusion.32
  18.1 0.3 convolution_convert_fusion
  18.4 0.7 fusion.45
  19.1 4.0 %collective-permute-start.12 = (bf16[8,3072]{1,0:T(8,128)(2,1)S(1)}, bf16[8,3072]{1,0:T(8,128)(2,1)S(1)}, u32[]{:S(2)}, u32[]{:S(2)}) collective-permute-start(bf16[8,3072]{1,0:T(8,128)(2,1)S(1)} %get-tuple-element.26), channel_id=1, source_target_pairs={{0,64},{1,65},{2,66},{3,67},{4,68},{5,69},{6,70},{7,71},{8,72},{9,... | collective-permute-start | bytes 147464 | tf_op jit(solution)/shard_map/ppermute | solution.py:41
  23.3 2.5 %collective-permute-start.13 = (bf16[8,3072]{1,0:T(8,128)(2,1)S(1)}, bf16[8,3072]{1,0:T(8,128)(2,1)S(1)}, u32[]{:S(2)}, u32[]{:S(2)}) collective-permute-start(bf16[8,3072]{1,0:T(8,128)(2,1)S(1)} %get-tuple-element.24), channel_id=1, source_target_pairs={{0,88},{1,89},{2,90},{3,91},{4,92},{5,93},{6,94},{7,95},{8,80},{9,... | collective-permute-start | bytes 147464 | tf_op jit(solution)/shard_map/ppermute | solution.py:41
  25.8 5.5 %collective-permute-start.6 = (bf16[8,3072]{1,0:T(8,128)(2,1)}, bf16[8,3072]{1,0:T(8,128)(2,1)S(1)}, u32[]{:S(2)}, u32[]{:S(2)}) collective-permute-start(bf16[8,3072]{1,0:T(8,128)(2,1)} %get-tuple-element.29), channel_id=1, source_target_pairs={{0,120},{1,121},{2,122},{3,123},{4,124},{5,125},{6,126},{7,127},{8... | collective-permute-start | bytes 147464 | tf_op jit(solution)/shard_map/ppermute | solution.py:41
  31.3 1.0 collective-permute-start.7
  32.4 1.2 collective-permute-done.6
  33.6 2.6 %collective-permute-start.8 = (bf16[8,3072]{1,0:T(8,128)(2,1)S(1)}, bf16[8,3072]{1,0:T(8,128)(2,1)S(1)}, u32[]{:S(2)}, u32[]{:S(2)}) collective-permute-start(bf16[8,3072]{1,0:T(8,128)(2,1)S(1)} %get-tuple-element.27), channel_id=1, source_target_pairs={{0,56},{1,57},{2,58},{3,59},{4,60},{5,61},{6,62},{7,63},{8,48},{9,... | collective-permute-start | bytes 147464 | tf_op jit(solution)/shard_map/ppermute | solution.py:41
  36.2 2.7 %collective-permute-start.1 = (bf16[8,3072]{1,0:T(8,128)(2,1)S(1)}, bf16[8,3072]{1,0:T(8,128)(2,1)S(1)}, u32[]{:S(2)}, u32[]{:S(2)}) collective-permute-start(bf16[8,3072]{1,0:T(8,128)(2,1)S(1)} %get-tuple-element.31), channel_id=1, source_target_pairs={{0,24},{1,25},{2,26},{3,27},{4,28},{5,29},{6,30},{7,31},{8,16},{9,... | collective-permute-start | bytes 147464 | tf_op jit(solution)/shard_map/ppermute | solution.py:41
  38.9 1.2 collective-permute-done.8
  40.0 3.3 %collective-permute-start.2 = (bf16[8,3072]{1,0:T(8,128)(2,1)S(1)}, bf16[8,3072]{1,0:T(8,128)(2,1)S(1)}, u32[]{:S(2)}, u32[]{:S(2)}) collective-permute-start(bf16[8,3072]{1,0:T(8,128)(2,1)S(1)} %get-tuple-element.30), channel_id=1, source_target_pairs={{0,96},{1,97},{2,98},{3,99},{4,100},{5,101},{6,102},{7,103},{8,104... | collective-permute-start | bytes 147464 | tf_op jit(solution)/shard_map/ppermute | solution.py:41
  43.4 2.8 %collective-permute-start.14 = (bf16[16,3072]{1,0:T(8,128)(2,1)S(1)}, bf16[16,3072]{1,0:T(8,128)(2,1)S(1)}, u32[]{:S(2)}, u32[]{:S(2)}) collective-permute-start(bf16[16,3072]{1,0:T(8,128)(2,1)S(1)} %pad_maximum_fusion.7), channel_id=1, source_target_pairs={{0,6},{1,7},{2,4},{3,5},{4,2},{5,3},{6,0},{7,1},{8,14},{9,15},{10,... | collective-permute-start | bytes 294920 | tf_op jit(solution)/shard_map/ppermute | solution.py:41
  46.2 0.7 collective-permute-start.9
  47.0 2.4 %collective-permute-done.14 = bf16[16,3072]{1,0:T(8,128)(2,1)S(1)} collective-permute-done((bf16[16,3072]{1,0:T(8,128)(2,1)S(1)}, bf16[16,3072]{1,0:T(8,128)(2,1)S(1)}, u32[]{:S(2)}, u32[]{:S(2)}) %collective-permute-start.14) | collective-permute-done | bytes 98336 | tf_op jit(solution)/shard_map/ppermute | solution.py:41
  49.3 0.8 pad_maximum_fusion.4
  50.2 1.3 %collective-permute-done.9 = bf16[24,3072]{1,0:T(8,128)(2,1)S(1)} collective-permute-done((bf16[24,3072]{1,0:T(8,128)(2,1)S(1)}, bf16[24,3072]{1,0:T(8,128)(2,1)S(1)}, u32[]{:S(2)}, u32[]{:S(2)}) %collective-permute-start.9) | collective-permute-done | bytes 147488 | tf_op jit(solution)/shard_map/ppermute | solution.py:41
  51.5 0.8 collective-permute-start.15
  52.3 2.2 %collective-permute-done.3 = bf16[24,3072]{1,0:T(8,128)(2,1)S(1)} collective-permute-done((bf16[24,3072]{1,0:T(8,128)(2,1)S(1)}, bf16[24,3072]{1,0:T(8,128)(2,1)S(1)}, u32[]{:S(2)}, u32[]{:S(2)}) %collective-permute-start.3) | collective-permute-done | bytes 147488 | tf_op jit(solution)/shard_map/ppermute | solution.py:41
  54.5 2.8 %collective-permute-start.10 = (bf16[48,3072]{1,0:T(8,128)(2,1)S(1)}, bf16[48,3072]{1,0:T(8,128)(2,1)S(1)}, u32[]{:S(2)}, u32[]{:S(2)}) collective-permute-start(bf16[48,3072]{1,0:T(8,128)(2,1)S(1)} %pad_maximum_fusion.3), channel_id=1, source_target_pairs={{0,6},{1,7},{2,4},{3,5},{4,2},{5,3},{6,0},{7,1},{8,14},{9,15},{10,... | collective-permute-start | bytes 884744 | tf_op jit(solution)/shard_map/ppermute | solution.py:41
  57.3 0.5 collective-permute-start.4
  57.7 5.0 %collective-permute-done.10 = bf16[48,3072]{1,0:T(8,128)(2,1)S(1)} collective-permute-done((bf16[48,3072]{1,0:T(8,128)(2,1)S(1)}, bf16[48,3072]{1,0:T(8,128)(2,1)S(1)}, u32[]{:S(2)}, u32[]{:S(2)}) %collective-permute-start.10) | collective-permute-done | bytes 294944 | tf_op jit(solution)/shard_map/ppermute | solution.py:41
  62.8 3.4 %collective-permute-done.4 = bf16[48,3072]{1,0:T(8,128)(2,1)S(1)} collective-permute-done((bf16[48,3072]{1,0:T(8,128)(2,1)S(1)}, bf16[48,3072]{1,0:T(8,128)(2,1)S(1)}, u32[]{:S(2)}, u32[]{:S(2)}) %collective-permute-start.4) | collective-permute-done | bytes 294944 | tf_op jit(solution)/shard_map/ppermute | solution.py:41
  66.3 0.5 collective-permute-start.11
  66.8 2.7 %collective-permute-start.5 = (bf16[96,3072]{1,0:T(8,128)(2,1)S(1)}, bf16[96,3072]{1,0:T(8,128)(2,1)S(1)}, u32[]{:S(2)}, u32[]{:S(2)}) collective-permute-start(bf16[96,3072]{1,0:T(8,128)(2,1)S(1)} %constant_dynamic-update-slice_fusion.refs_0_), channel_id=1, source_target_pairs={{0,6},{1,7},{2,4},{3,5},{4,2},{5,3},{6,0},{7,1},{8,14},{9,15},{10,... | collective-permute-start | bytes 1769480 | tf_op jit(solution)/shard_map/ppermute | solution.py:41
  69.5 4.5 %load.1 = (bf16[672,3072]{1,0:T(8,128)(2,1)S(1)}, bf16[672,3072]{1,0:T(8,128)(2,1)S(1)}, bf16[672,3072]{1,0:T(8,128)(2,1)S(1)}) custom-call(bf16[336,3072]{1,0:T(8,128)(2,1)S(1)} %bitcast.24, bf16[336,3072]{1,0:T(8,128)(2,1)} %collective-permute-done.17.refs_1_, bf16[336,3072]{1,0:T(8,128)(2,1)} %bitcast.5.refs_2_, ...), custom_call_target="tpu_custom_call" | custom-call | flops 12683575296 | bytes 12386304 | tf_op jit(solution)/shard_map/load/pallas_call | solution.py:73
  74.0 5.9 %experts.2.refs_6_ = bf16[64,8,3072]{2,1,0:T(8,128)(2,1)} custom-call(s32[32]{0:T(128)S(1)} %get-tuple-element.41.targets, bf16[96,3072]{1,0:T(8,128)(2,1)S(1)} %constant_dynamic-update-slice_fusion.refs_0_, bf16[96,3072]{1,0:T(8,128)(2,1)S(1)} %constant_dynamic-update-slice_fusion.5.refs_1_, ...), custom_call_target="tpu_custom_call" | custom-call | flops 3170893824 | bytes 3145728 | tf_op jit(solution)/shard_map/experts/pallas_call | solution.py:137
  79.9 5.9 %experts.3 = bf16[64,8,3072]{2,1,0:T(8,128)(2,1)} custom-call(s32[32]{0:T(128)S(1)} %get-tuple-element.42.targets, bf16[96,3072]{1,0:T(8,128)(2,1)S(1)} %collective-permute-done.5.refs_0_, bf16[96,3072]{1,0:T(8,128)(2,1)S(1)} %collective-permute-done.11.refs_1_, ...), custom_call_target="tpu_custom_call", output_to_operand_aliasing={{}: (7, {})} | custom-call | flops 3170893824 | bytes 3145728 | tf_op jit(solution)/shard_map/experts/pallas_call | solution.py:137
  85.8 6.5 %all-to-all-start = ((bf16[64,8,3072]{2,1,0:T(8,128)(2,1)}), bf16[64,8,3072]{2,1,0:T(8,128)(2,1)S(1)}, u32[]{:S(2)}, u32[]{:S(2)}) async-start(bf16[64,8,3072]{2,1,0:T(8,128)(2,1)} %experts.3), calls=%async_computation | async-start | bytes 6291456 | tf_op jit(solution)/shard_map/all_to_all | solution.py:300
  92.3 2.5 %pad_maximum_fusion.1 = f32[32,48,128]{2,1,0:T(8,128)} fusion(f32[32,48,64]{2,1,0:T(8,128)} %get-tuple-element.23, f32[32,48,64]{2,1,0:T(8,128)} %subtract_add_fusion), kind=kLoop, calls=%fused_computation.5 | loop fusion | flops 196608 | bytes 1572864 | tf_op jit(solution)/shard_map/concatenate | solution.py:213
  94.9 1.4 %broadcast_multiply_fusion = f32[64,64]{0,1:T(8,128)} fusion(f32[64,64]{0,1:T(8,128)} %fusion.32, f32[64]{0:T(128)S(1)} %reshape.141), kind=kLoop, calls=%fused_computation.78 | loop fusion | flops 4096 | bytes 33024 | tf_op jit(solution)/shard_map/mul | solution.py:306
  96.3 0.8 reduce_sum.68
  97.1 28.7 %all-to-all-done = bf16[64,8,3072]{2,1,0:T(8,128)(2,1)S(1)} async-done(((bf16[64,8,3072]{2,1,0:T(8,128)(2,1)}), bf16[64,8,3072]{2,1,0:T(8,128)(2,1)S(1)}, u32[]{:S(2)}, u32[]{:S(2)}) %all-to-all-start) | async-done | bytes 3145760 | tf_op jit(solution)/shard_map/all_to_all | solution.py:300
  125.8 0.5 convert_reduce_fusion
  126.7 1.4 %collective-permute-done.20 = f32[32,1536]{1,0:T(8,128)S(1)} collective-permute-done((f32[32,1536]{1,0:T(8,128)S(1)}, f32[32,1536]{1,0:T(8,128)S(1)}, u32[]{:S(2)}, u32[]{:S(2)}) %collective-permute-start.20) | collective-permute-done | bytes 196640 | tf_op jit(solution)/shard_map/ppermute | solution.py:53
  128.1 0.7 add_convert_fusion
  (86 shorter events, 2.6 us)
Async XLA Ops:
  0.6 5.5 %copy-start = (bf16[48,128,16]{1,2,0:T(8,128)(2,1)S(1)}, bf16[48,128,16]{1,2,0:T(8,128)(2,1)}, u32[]{:S(2)}) copy-start(bf16[48,128,16]{1,2,0:T(8,128)(2,1)} %param.23) | copy-start | bytes 589828
  0.6 6.3 %copy-start.7 = (f32[48,64]{1,0:T(8,128)S(1)}, f32[48,64]{1,0:T(8,128)}, u32[]{:S(2)}) copy-start(f32[48,64]{1,0:T(8,128)} %param.20) | copy-start | bytes 36868
  0.7 6.3 %copy-start.6 = (f32[48,64]{1,0:T(8,128)S(1)}, f32[48,64]{1,0:T(8,128)}, u32[]{:S(2)}) copy-start(f32[48,64]{1,0:T(8,128)} %param.21) | copy-start | bytes 36868
  1.4 5.8 %copy-start.2 = (f32[32,48,128]{2,1,0:T(8,128)S(1)}, f32[32,48,128]{2,1,0:T(8,128)}, u32[]{:S(2)}) copy-start(f32[32,48,128]{2,1,0:T(8,128)} %param.19) | copy-start | bytes 2359300
  7.2 4.3 %copy-start.5 = (bf16[48,16,128]{2,1,0:T(8,128)(2,1)S(1)}, bf16[48,16,128]{2,1,0:T(8,128)(2,1)}, u32[]{:S(2)}) copy-start(bf16[48,16,128]{2,1,0:T(8,128)(2,1)} %param.24) | copy-start | bytes 589828
  8.6 3.4 %copy-start.9 = (f32[768]{0:T(1024)S(1)}, f32[768]{0:T(1024)}, u32[]{:S(2)}) copy-start(f32[768]{0:T(1024)} %param.25) | copy-start | bytes 9220
  9.9 5.3 %copy-start.1 = (bf16[3072,336]{0,1:T(8,128)(2,1)S(1)}, bf16[3072,336]{0,1:T(8,128)(2,1)}, u32[]{:S(2)}) copy-start(bf16[3072,336]{0,1:T(8,128)(2,1)} %param.32) | copy-start | bytes 6193156
  9.9 6.3 %copy-start.10 = (s32[32,2]{0,1:T(2,128)S(1)}, s32[32,2]{0,1:T(2,128)}, u32[]{:S(2)}) copy-start(s32[32,2]{0,1:T(2,128)} %param.30) | copy-start | bytes 772
  9.9 7.8 %copy-start.11 = (f32[32,2]{0,1:T(2,128)S(1)}, f32[32,2]{0,1:T(2,128)}, u32[]{:S(2)}) copy-start(f32[32,2]{0,1:T(2,128)} %param.31) | copy-start | bytes 772
  9.9 7.9 %copy-start.12 = (s32[64]{0:T(128)S(1)}, s32[64]{0:T(128)}, u32[]{:S(2)}) copy-start(s32[64]{0:T(128)} %constant.124.clone) | copy-start | bytes 772
  9.9 8.0 %copy-start.3 = (bf16[32,3072]{1,0:T(8,128)(2,1)S(1)}, bf16[32,3072]{1,0:T(8,128)(2,1)}, u32[]{:S(2)}) copy-start(bf16[32,3072]{1,0:T(8,128)(2,1)} %param.18) | copy-start | bytes 589828
  11.5 6.7 %copy-start.8 = (f32[3072]{0:T(1024)S(1)}, f32[3072]{0:T(1024)}, u32[]{:S(2)}) copy-start(f32[3072]{0:T(1024)} %param.29) | copy-start | bytes 36868
  15.2 2.7 %collective-permute-start = (bf16[32,3072]{1,0:T(8,128)(2,1)S(1)}, bf16[32,3072]{1,0:T(8,128)(2,1)S(1)}, u32[]{:S(2)}, u32[]{:S(2)}) collective-permute-start(bf16[32,3072]{1,0:T(8,128)(2,1)S(1)} %convolution_convert_fusion.1), channel_id=1, source_target_pairs={{0,1},{1,0},{2,3},{3,2},{4,5},{5,4},{6,7},{7,6},{8,9},{9,8},{10,11... | collective-permute-start | bytes 589832 | tf_op jit(solution)/shard_map/ppermute | solution.py:53
  15.2 51.6 %collective-permute-start.17 = (bf16[336,3072]{1,0:T(8,128)(2,1)S(1)}, bf16[336,3072]{1,0:T(8,128)(2,1)}, u32[]{:S(2)}, u32[]{:S(2)}) collective-permute-start(bf16[336,3072]{1,0:T(8,128)(2,1)S(1)} %bitcast.23), channel_id=1, source_target_pairs={{0,1},{1,0},{2,3},{3,2},{4,5},{5,4},{6,7},{7,6},{8,9},{9,8},{10,11... | collective-permute-start | bytes 6193160 | tf_op jit(solution)/shard_map/ppermute | solution.py:53
  15.7 53.8 %collective-permute-start.18 = (bf16[336,3072]{1,0:T(8,128)(2,1)}, bf16[336,3072]{1,0:T(8,128)(2,1)}, u32[]{:S(2)}, u32[]{:S(2)}) collective-permute-start(bf16[336,3072]{1,0:T(8,128)(2,1)} %bitcast.5.refs_2_), channel_id=1, source_target_pairs={{0,1},{1,0},{2,3},{3,2},{4,5},{5,4},{6,7},{7,6},{8,9},{9,8},{10,11... | collective-permute-start | bytes 6193160 | tf_op jit(solution)/shard_map/ppermute | solution.py:53
  15.8 53.7 %collective-permute-start.19 = (bf16[336,3072]{1,0:T(8,128)(2,1)}, bf16[336,3072]{1,0:T(8,128)(2,1)}, u32[]{:S(2)}, u32[]{:S(2)}) collective-permute-start(bf16[336,3072]{1,0:T(8,128)(2,1)} %refs_4_.1), channel_id=1, source_target_pairs={{0,1},{1,0},{2,3},{3,2},{4,5},{5,4},{6,7},{7,6},{8,9},{9,8},{10,11... | collective-permute-start | bytes 6193160 | tf_op jit(solution)/shard_map/ppermute | solution.py:53
  19.1 6.7 %collective-permute-start.12 = (bf16[8,3072]{1,0:T(8,128)(2,1)S(1)}, bf16[8,3072]{1,0:T(8,128)(2,1)S(1)}, u32[]{:S(2)}, u32[]{:S(2)}) collective-permute-start(bf16[8,3072]{1,0:T(8,128)(2,1)S(1)} %get-tuple-element.26), channel_id=1, source_target_pairs={{0,64},{1,65},{2,66},{3,67},{4,68},{5,69},{6,70},{7,71},{8,72},{9,... | collective-permute-start | bytes 147464 | tf_op jit(solution)/shard_map/ppermute | solution.py:41
  23.3 8.0 %collective-permute-start.13 = (bf16[8,3072]{1,0:T(8,128)(2,1)S(1)}, bf16[8,3072]{1,0:T(8,128)(2,1)S(1)}, u32[]{:S(2)}, u32[]{:S(2)}) collective-permute-start(bf16[8,3072]{1,0:T(8,128)(2,1)S(1)} %get-tuple-element.24), channel_id=1, source_target_pairs={{0,88},{1,89},{2,90},{3,91},{4,92},{5,93},{6,94},{7,95},{8,80},{9,... | collective-permute-start | bytes 147464 | tf_op jit(solution)/shard_map/ppermute | solution.py:41
  25.8 21.1 %copy-start.4 = (bf16[8,3072]{1,0:T(8,128)(2,1)}, bf16[8,3072]{1,0:T(8,128)(2,1)S(1)}, u32[]{:S(2)}) copy-start(bf16[8,3072]{1,0:T(8,128)(2,1)S(1)} %collective-permute-done.12) | copy-start | bytes 147460
  25.8 7.7 %collective-permute-start.6 = (bf16[8,3072]{1,0:T(8,128)(2,1)}, bf16[8,3072]{1,0:T(8,128)(2,1)S(1)}, u32[]{:S(2)}, u32[]{:S(2)}) collective-permute-start(bf16[8,3072]{1,0:T(8,128)(2,1)} %get-tuple-element.29), channel_id=1, source_target_pairs={{0,120},{1,121},{2,122},{3,123},{4,124},{5,125},{6,126},{7,127},{8... | collective-permute-start | bytes 147464 | tf_op jit(solution)/shard_map/ppermute | solution.py:41
  31.3 4.8 %collective-permute-start.7 = (bf16[8,3072]{1,0:T(8,128)(2,1)}, bf16[8,3072]{1,0:T(8,128)(2,1)S(1)}, u32[]{:S(2)}, u32[]{:S(2)}) collective-permute-start(bf16[8,3072]{1,0:T(8,128)(2,1)} %get-tuple-element.28), channel_id=1, source_target_pairs={{0,32},{1,33},{2,34},{3,35},{4,36},{5,37},{6,38},{7,39},{8,40},{9,... | collective-permute-start | bytes 147464 | tf_op jit(solution)/shard_map/ppermute | solution.py:41
  33.6 6.5 %collective-permute-start.8 = (bf16[8,3072]{1,0:T(8,128)(2,1)S(1)}, bf16[8,3072]{1,0:T(8,128)(2,1)S(1)}, u32[]{:S(2)}, u32[]{:S(2)}) collective-permute-start(bf16[8,3072]{1,0:T(8,128)(2,1)S(1)} %get-tuple-element.27), channel_id=1, source_target_pairs={{0,56},{1,57},{2,58},{3,59},{4,60},{5,61},{6,62},{7,63},{8,48},{9,... | collective-permute-start | bytes 147464 | tf_op jit(solution)/shard_map/ppermute | solution.py:41
  36.2 7.2 %collective-permute-start.1 = (bf16[8,3072]{1,0:T(8,128)(2,1)S(1)}, bf16[8,3072]{1,0:T(8,128)(2,1)S(1)}, u32[]{:S(2)}, u32[]{:S(2)}) collective-permute-start(bf16[8,3072]{1,0:T(8,128)(2,1)S(1)} %get-tuple-element.31), channel_id=1, source_target_pairs={{0,24},{1,25},{2,26},{3,27},{4,28},{5,29},{6,30},{7,31},{8,16},{9,... | collective-permute-start | bytes 147464 | tf_op jit(solution)/shard_map/ppermute | solution.py:41
  40.0 6.2 %collective-permute-start.2 = (bf16[8,3072]{1,0:T(8,128)(2,1)S(1)}, bf16[8,3072]{1,0:T(8,128)(2,1)S(1)}, u32[]{:S(2)}, u32[]{:S(2)}) collective-permute-start(bf16[8,3072]{1,0:T(8,128)(2,1)S(1)} %get-tuple-element.30), channel_id=1, source_target_pairs={{0,96},{1,97},{2,98},{3,99},{4,100},{5,101},{6,102},{7,103},{8,104... | collective-permute-start | bytes 147464 | tf_op jit(solution)/shard_map/ppermute | solution.py:41
  43.4 5.9 %collective-permute-start.14 = (bf16[16,3072]{1,0:T(8,128)(2,1)S(1)}, bf16[16,3072]{1,0:T(8,128)(2,1)S(1)}, u32[]{:S(2)}, u32[]{:S(2)}) collective-permute-start(bf16[16,3072]{1,0:T(8,128)(2,1)S(1)} %pad_maximum_fusion.7), channel_id=1, source_target_pairs={{0,6},{1,7},{2,4},{3,5},{4,2},{5,3},{6,0},{7,1},{8,14},{9,15},{10,... | collective-permute-start | bytes 294920 | tf_op jit(solution)/shard_map/ppermute | solution.py:41
  46.2 5.2 %collective-permute-start.9 = (bf16[24,3072]{1,0:T(8,128)(2,1)S(1)}, bf16[24,3072]{1,0:T(8,128)(2,1)S(1)}, u32[]{:S(2)}, u32[]{:S(2)}) collective-permute-start(bf16[24,3072]{1,0:T(8,128)(2,1)S(1)} %pad_maximum_fusion.6), channel_id=1, source_target_pairs={{0,2},{1,3},{2,0},{3,1},{4,6},{5,7},{6,4},{7,5},{8,10},{9,11},{10,... | collective-permute-start | bytes 442376 | tf_op jit(solution)/shard_map/ppermute | solution.py:41
  49.3 5.1 %collective-permute-start.3 = (bf16[24,3072]{1,0:T(8,128)(2,1)S(1)}, bf16[24,3072]{1,0:T(8,128)(2,1)S(1)}, u32[]{:S(2)}, u32[]{:S(2)}) collective-permute-start(bf16[24,3072]{1,0:T(8,128)(2,1)S(1)} %pad_maximum_fusion.5), channel_id=1, source_target_pairs={{0,8},{1,9},{2,10},{3,11},{4,12},{5,13},{6,14},{7,15},{8,0},{9,1},... | collective-permute-start | bytes 442376 | tf_op jit(solution)/shard_map/ppermute | solution.py:41
  51.5 5.8 %collective-permute-start.15 = (bf16[32,3072]{1,0:T(8,128)(2,1)S(1)}, bf16[32,3072]{1,0:T(8,128)(2,1)S(1)}, u32[]{:S(2)}, u32[]{:S(2)}) collective-permute-start(bf16[32,3072]{1,0:T(8,128)(2,1)S(1)} %pad_maximum_fusion.4), channel_id=1, source_target_pairs={{0,8},{1,9},{2,10},{3,11},{4,12},{5,13},{6,14},{7,15},{8,0},{9,1},... | collective-permute-start | bytes 589832 | tf_op jit(solution)/shard_map/ppermute | solution.py:41
  54.5 8.3 %collective-permute-start.10 = (bf16[48,3072]{1,0:T(8,128)(2,1)S(1)}, bf16[48,3072]{1,0:T(8,128)(2,1)S(1)}, u32[]{:S(2)}, u32[]{:S(2)}) collective-permute-start(bf16[48,3072]{1,0:T(8,128)(2,1)S(1)} %pad_maximum_fusion.3), channel_id=1, source_target_pairs={{0,6},{1,7},{2,4},{3,5},{4,2},{5,3},{6,0},{7,1},{8,14},{9,15},{10,... | collective-permute-start | bytes 884744 | tf_op jit(solution)/shard_map/ppermute | solution.py:41
  57.3 9.0 %collective-permute-start.4 = (bf16[48,3072]{1,0:T(8,128)(2,1)S(1)}, bf16[48,3072]{1,0:T(8,128)(2,1)S(1)}, u32[]{:S(2)}, u32[]{:S(2)}) collective-permute-start(bf16[48,3072]{1,0:T(8,128)(2,1)S(1)} %pad_maximum_fusion.2), channel_id=1, source_target_pairs={{0,2},{1,3},{2,0},{3,1},{4,6},{5,7},{6,4},{7,5},{8,10},{9,11},{10,... | collective-permute-start | bytes 884744 | tf_op jit(solution)/shard_map/ppermute | solution.py:41
  62.8 17.1 %collective-permute-start.16 = (bf16[64,3072]{1,0:T(8,128)(2,1)S(1)}, bf16[64,3072]{1,0:T(8,128)(2,1)S(1)}, u32[]{:S(2)}, u32[]{:S(2)}) collective-permute-start(bf16[64,3072]{1,0:T(8,128)(2,1)S(1)} %constant_dynamic-update-slice_fusion.10.refs_6_.refs_2_), channel_id=1, source_target_pairs={{0,2},{1,3},{2,0},{3,1},{4,6},{5,7},{6,4},{7,5},{8,10},{9,11},{10,... | collective-permute-start | bytes 1179656 | tf_op jit(solution)/shard_map/ppermute | solution.py:41
  66.3 13.7 %collective-permute-start.11 = (bf16[96,3072]{1,0:T(8,128)(2,1)S(1)}, bf16[96,3072]{1,0:T(8,128)(2,1)S(1)}, u32[]{:S(2)}, u32[]{:S(2)}) collective-permute-start(bf16[96,3072]{1,0:T(8,128)(2,1)S(1)} %constant_dynamic-update-slice_fusion.5.refs_1_), channel_id=1, source_target_pairs={{0,8},{1,9},{2,10},{3,11},{4,12},{5,13},{6,14},{7,15},{8,0},{9,1},... | collective-permute-start | bytes 1769480 | tf_op jit(solution)/shard_map/ppermute | solution.py:41
  66.8 13.2 %collective-permute-start.5 = (bf16[96,3072]{1,0:T(8,128)(2,1)S(1)}, bf16[96,3072]{1,0:T(8,128)(2,1)S(1)}, u32[]{:S(2)}, u32[]{:S(2)}) collective-permute-start(bf16[96,3072]{1,0:T(8,128)(2,1)S(1)} %constant_dynamic-update-slice_fusion.refs_0_), channel_id=1, source_target_pairs={{0,6},{1,7},{2,4},{3,5},{4,2},{5,3},{6,0},{7,1},{8,14},{9,15},{10,... | collective-permute-start | bytes 1769480 | tf_op jit(solution)/shard_map/ppermute | solution.py:41
  85.8 40.0 %all-to-all-start = ((bf16[64,8,3072]{2,1,0:T(8,128)(2,1)}), bf16[64,8,3072]{2,1,0:T(8,128)(2,1)S(1)}, u32[]{:S(2)}, u32[]{:S(2)}) async-start(bf16[64,8,3072]{2,1,0:T(8,128)(2,1)} %experts.3), calls=%async_computation | async-start | bytes 6291456 | tf_op jit(solution)/shard_map/all_to_all | solution.py:300
  126.6 1.5 %collective-permute-start.20 = (f32[32,1536]{1,0:T(8,128)S(1)}, f32[32,1536]{1,0:T(8,128)S(1)}, u32[]{:S(2)}, u32[]{:S(2)}) collective-permute-start(f32[32,1536]{1,0:T(8,128)S(1)} %constant_dynamic-slice_fusion), channel_id=1, source_target_pairs={{0,1},{1,0},{2,3},{3,2},{4,5},{5,4},{6,7},{7,6},{8,9},{9,8},{10,11... | collective-permute-start | bytes 589832 | tf_op jit(solution)/shard_map/ppermute | solution.py:53
where the time goes:
time: 130 us; the launch traced here: 129 us
  waiting for transfers between devices  46.9 us (36%)
  starting transfers between devices  40 us (31%)
  Pallas kernels  16.3 us (13%)
  other arithmetic  13.8 us (11%)
  matrix products  7.8 us (6%)
  local copies, waits for them, and re-layouts  2.99 us (2%)
    ppermute x16, starting transfers between devices, over_links(): return lax.ppermute(shard, ('ep', 'tp'), pairs)  32.3 us
    all_to_all x1, waiting for transfers between devices, per_device(): lax.all_to_all(produced, 'ep', split_axis=0, concat_axis=0, tiled=True)  28.7 us
    ppermute x16, waiting for transfers between devices, over_links(): return lax.ppermute(shard, ('ep', 'tp'), pairs)  16.7 us
    pallas_call x2, Pallas kernels, experts(): pl.pallas_call(lambda targets, *refs: expert_kernel(sizes, targets, *refs...  11.8 us
    all_to_all x1, starting transfers between devices, per_device(): lax.all_to_all(produced, 'ep', split_axis=0, concat_axis=0, tiled=True)  6.51 us
    pallas_call x1, Pallas kernels, loaded(): pl.pallas_call(lambda *refs: load_kernel(units, *refs), out_shape=[pltpu....  4.48 us
    dot_general x1, matrix products, per_device(): jnp.dot(normed, w_in, preferred_element_type=jnp.float32)  3.43 us
    dot_general x1, matrix products, per_device(): jnp.dot(activated, w_out, preferred_element_type=jnp.float32)  3.22 us
  transfers between devices with their start and end apart: 22, of which 9 were waited for; matrix products, arithmetic and copies ran while one was open for 7% of the time, Pallas kernels for 8%

commit v1 on v0

--- a/solution.py
+++ b/solution.py
@@ -286,7 +286,7 @@
             across = over_links(rows, spread_links(step, colour))
             rows = jnp.concatenate([rows, across], axis=0)
         near.append(rows)
-    held_units = loaded(gates, ups, downs, near[-1:])
+    held_units = loaded(gates, ups, downs, ())
     far = []
     for colour, rows in enumerate(near):
         far.append(over_links(rows, spread_links(2, colour)))
@@ -294,9 +294,6 @@
     half = targets.shape[0] // 2
     produced = experts(near, targets[:half], held_units, slots)
     produced = experts(far, targets[half:], held_units, slots, (produced,))
-    produced, weights_flat, placement = lax.optimization_barrier(
-        (produced, weights_flat, placement)
-    )
     returned = lax.all_to_all(produced, "ep", split_axis=0, concat_axis=0, tiled=True)
     new_carried = with_layout_constraint(new_carried, Layout(major_to_minor=(0, 1, 2)))
     returned, new_carried = lax.optimization_barrier((returned, new_carried))

time: 130 us -> 129 us (level)
  other arithmetic: 13.8 us -> 11.6 us
  waiting for transfers between devices: 46.9 us -> 48.6 us
    mul x1 -> x2, other arithmetic: 1.45 us -> 0.01 us  [the longest x1 0.01 us: per_device(): sent_to = jnp.where(held, block * slots + slot_index, -1)]
    ppermute x16, waiting for transfers between devices: 16.7 us -> 18 us  [over_links(): return lax.ppermute(shard, ('ep', 'tp'), pairs)]
  transfers between devices with their start and end apart: 22 -> 22, of which waited for: 9 -> 9; matrix products, arithmetic and copies ran while one was open for 7% -> 5% of each run, Pallas kernels for 8% -> 8%
where the time goes in v1:
time: 129 us; the launch traced here: 127 us
  waiting for transfers between devices  48.6 us (38%)
  starting transfers between devices  38.9 us (30%)
  Pallas kernels  16.4 us (13%)
  other arithmetic  11.6 us (9%)
  matrix products  7.8 us (6%)
  local copies, waits for them, and re-layouts  2.97 us (2%)
    ppermute x16, starting transfers between devices, over_links(): return lax.ppermute(shard, ('ep', 'tp'), pairs)  31.9 us
    all_to_all x1, waiting for transfers between devices, per_device(): lax.all_to_all(produced, 'ep', split_axis=0, concat_axis=0, tiled=True)  29.1 us
    ppermute x16, waiting for transfers between devices, over_links(): return lax.ppermute(shard, ('ep', 'tp'), pairs)  18 us
    pallas_call x2, Pallas kernels, experts(): pl.pallas_call(lambda targets, *refs: expert_kernel(sizes, targets, *refs...  11.9 us
    all_to_all x1, starting transfers between devices, per_device(): lax.all_to_all(produced, 'ep', split_axis=0, concat_axis=0, tiled=True)  5.91 us
    pallas_call x1, Pallas kernels, loaded(): pl.pallas_call(lambda *refs: load_kernel(units, *refs), out_shape=[pltpu....  4.48 us
    dot_general x1, matrix products, per_device(): jnp.dot(normed, w_in, preferred_element_type=jnp.float32)  3.43 us
    dot_general x1, matrix products, per_device(): jnp.dot(activated, w_out, preferred_element_type=jnp.float32)  3.22 us
  transfers between devices with their start and end apart: 22, of which 9 were waited for; matrix products, arithmetic and copies ran while one was open for 5% of the time, Pallas kernels for 8%

profile of v1, /device:TPU:0, one launch (start us, length us, event | category | flops | bytes accessed | tf_op | source)
XLA Modules:
  0.0 127.3 jit_solution(289256754438914933)
XLA Ops:
  0.7 0.7 exp.14
  1.4 1.1 fusion.7
  2.5 3.4 %convolution_convert_fusion.2 = bf16[32,768]{1,0:T(8,128)(2,1)S(1)} fusion(bf16[3072,768]{1,0:T(8,128)(2,1)} %param.27, bf16[32,3072]{1,0:T(8,128)(2,1)} %param.18, f32[3072]{0:T(1024)} %param.26, f32[32]{0:T(128)S(1)} %add_rsqrt_fusion.1), kind=kOutput, calls=%fused_computation.3 | convolution fusion | flops 151412736 | bytes 4976768 | tf_op jit(solution)/shard_map/dot_general | solution.py:245
  6.1 0.3 fusion.46
  6.5 0.5 copy.50
  7.0 0.2 cosine_multiply_fusion
  7.2 1.4 %fusion.43 = (bf16[32,48,64]{2,1,0:T(8,128)(2,1)S(1)}, f32[32,48,64]{2,1,0:T(8,128)}) fusion(f32[32,48,128]{2,1,0:T(8,128)S(1)} %bitcast.24, f32[48,64]{1,0:T(8,128)S(1)} %get-tuple-element.29, f32[48,64]{1,0:T(8,128)S(1)} %get-tuple-element.30, f32[32,48,128]{2,1,0:T(8,128)S(1)} %copy-done.2, f32[48,64]{1,0:T(8,128)S(1)} %get-tuple-element.28, ...), kind=kLoop, calls=%fused_computation.107 | loop fusion | flops 884736 | bytes 2211840 | tf_op jit(solution)/shard_map/neg | solution.py:209
  8.6 1.4 %subtract_add_fusion = f32[32,48,64]{2,1,0:T(8,128)} fusion(f32[32,48,128]{2,1,0:T(8,128)S(1)} %bitcast.25, f32[32,48,128]{2,1,0:T(8,128)S(1)} %copy-done.2, f32[48,64]{1,0:T(8,128)S(1)} %get-tuple-element.29, f32[48,64]{1,0:T(8,128)S(1)} %get-tuple-element.30, f32[48,64]{1,0:T(8,128)S(1)} %get-tuple-element.28, f32[48,64]{1,0:T(8,128)S(1)} %get-tuple-element.27), kind=kLoop, calls=%fused_computation.12 | loop fusion | flops 688128 | bytes 2015232 | tf_op jit(solution)/shard_map/add | solution.py:207
  10.0 1.5 %pad_maximum_fusion = bf16[32,48,128]{2,1,0:T(8,128)(2,1)S(1)} fusion(bf16[32,48,64]{2,1,0:T(8,128)(2,1)S(1)} %get-tuple-element.16, f32[32,48,64]{2,1,0:T(8,128)} %subtract_add_fusion), kind=kLoop, calls=%fused_computation.4 | loop fusion | flops 786432 | bytes 983040 | tf_op jit(solution)/shard_map/concatenate | solution.py:209
  11.5 0.3 fusion.2
  11.9 3.2 %convolution_convert_fusion.1 = bf16[32,3072]{1,0:T(8,128)(2,1)S(1)} fusion(bf16[768,3072]{1,0:T(8,128)(2,1)} %param.28, f32[32,768]{1,0:T(8,128)S(1)} %copy.40, bf16[32,768]{1,0:T(8,128)(2,1)S(1)} %convolution_convert_fusion.2, f32[768]{0:T(1024)S(1)} %copy-done.9), kind=kOutput, calls=%fused_computation.2 | convolution fusion | flops 151388160 | bytes 5065728 | tf_op jit(solution)/shard_map/dot_general | solution.py:249
  15.2 0.5 collective-permute-start.17
  15.8 0.4 collective-permute-start.19
  17.3 0.2 fusion.4
  17.6 0.3 convolution_convert_fusion
  17.9 4.1 %collective-permute-start.12 = (bf16[8,3072]{1,0:T(8,128)(2,1)S(1)}, bf16[8,3072]{1,0:T(8,128)(2,1)S(1)}, u32[]{:S(2)}, u32[]{:S(2)}) collective-permute-start(bf16[8,3072]{1,0:T(8,128)(2,1)S(1)} %get-tuple-element.20), channel_id=1, source_target_pairs={{0,64},{1,65},{2,66},{3,67},{4,68},{5,69},{6,70},{7,71},{8,72},{9,... | collective-permute-start | bytes 147464 | tf_op jit(solution)/shard_map/ppermute | solution.py:41
  22.1 2.5 %collective-permute-start.13 = (bf16[8,3072]{1,0:T(8,128)(2,1)S(1)}, bf16[8,3072]{1,0:T(8,128)(2,1)S(1)}, u32[]{:S(2)}, u32[]{:S(2)}) collective-permute-start(bf16[8,3072]{1,0:T(8,128)(2,1)S(1)} %get-tuple-element.18), channel_id=1, source_target_pairs={{0,88},{1,89},{2,90},{3,91},{4,92},{5,93},{6,94},{7,95},{8,80},{9,... | collective-permute-start | bytes 147464 | tf_op jit(solution)/shard_map/ppermute | solution.py:41
  24.6 5.6 %collective-permute-start.6 = (bf16[8,3072]{1,0:T(8,128)(2,1)S(1)}, bf16[8,3072]{1,0:T(8,128)(2,1)S(1)}, u32[]{:S(2)}, u32[]{:S(2)}) collective-permute-start(bf16[8,3072]{1,0:T(8,128)(2,1)S(1)} %get-tuple-element.23), channel_id=1, source_target_pairs={{0,120},{1,121},{2,122},{3,123},{4,124},{5,125},{6,126},{7,127},{8... | collective-permute-start | bytes 147464 | tf_op jit(solution)/shard_map/ppermute | solution.py:41
  30.2 1.0 collective-permute-start.7
  31.3 1.0 collective-permute-done.6
  32.3 2.6 %collective-permute-start.8 = (bf16[8,3072]{1,0:T(8,128)(2,1)S(1)}, bf16[8,3072]{1,0:T(8,128)(2,1)S(1)}, u32[]{:S(2)}, u32[]{:S(2)}) collective-permute-start(bf16[8,3072]{1,0:T(8,128)(2,1)S(1)} %get-tuple-element.21), channel_id=1, source_target_pairs={{0,56},{1,57},{2,58},{3,59},{4,60},{5,61},{6,62},{7,63},{8,48},{9,... | collective-permute-start | bytes 147464 | tf_op jit(solution)/shard_map/ppermute | solution.py:41
  34.8 2.5 %collective-permute-start.1 = (bf16[8,3072]{1,0:T(8,128)(2,1)S(1)}, bf16[8,3072]{1,0:T(8,128)(2,1)S(1)}, u32[]{:S(2)}, u32[]{:S(2)}) collective-permute-start(bf16[8,3072]{1,0:T(8,128)(2,1)S(1)} %get-tuple-element.25), channel_id=1, source_target_pairs={{0,24},{1,25},{2,26},{3,27},{4,28},{5,29},{6,30},{7,31},{8,16},{9,... | collective-permute-start | bytes 147464 | tf_op jit(solution)/shard_map/ppermute | solution.py:41
  37.4 1.4 %collective-permute-done.8 = bf16[8,3072]{1,0:T(8,128)(2,1)S(1)} collective-permute-done((bf16[8,3072]{1,0:T(8,128)(2,1)S(1)}, bf16[8,3072]{1,0:T(8,128)(2,1)S(1)}, u32[]{:S(2)}, u32[]{:S(2)}) %collective-permute-start.8) | collective-permute-done | bytes 49184 | tf_op jit(solution)/shard_map/ppermute | solution.py:41
  38.7 3.1 %collective-permute-start.2 = (bf16[8,3072]{1,0:T(8,128)(2,1)S(1)}, bf16[8,3072]{1,0:T(8,128)(2,1)S(1)}, u32[]{:S(2)}, u32[]{:S(2)}) collective-permute-start(bf16[8,3072]{1,0:T(8,128)(2,1)S(1)} %get-tuple-element.24), channel_id=1, source_target_pairs={{0,96},{1,97},{2,98},{3,99},{4,100},{5,101},{6,102},{7,103},{8,104... | collective-permute-start | bytes 147464 | tf_op jit(solution)/shard_map/ppermute | solution.py:41
  41.9 2.8 %collective-permute-start.14 = (bf16[16,3072]{1,0:T(8,128)(2,1)S(1)}, bf16[16,3072]{1,0:T(8,128)(2,1)S(1)}, u32[]{:S(2)}, u32[]{:S(2)}) collective-permute-start(bf16[16,3072]{1,0:T(8,128)(2,1)S(1)} %pad_maximum_fusion.7), channel_id=1, source_target_pairs={{0,6},{1,7},{2,4},{3,5},{4,2},{5,3},{6,0},{7,1},{8,14},{9,15},{10,... | collective-permute-start | bytes 294920 | tf_op jit(solution)/shard_map/ppermute | solution.py:41
  44.7 0.8 collective-permute-start.9
  45.6 2.2 %collective-permute-done.14 = bf16[16,3072]{1,0:T(8,128)(2,1)S(1)} collective-permute-done((bf16[16,3072]{1,0:T(8,128)(2,1)S(1)}, bf16[16,3072]{1,0:T(8,128)(2,1)S(1)}, u32[]{:S(2)}, u32[]{:S(2)}) %collective-permute-start.14) | collective-permute-done | bytes 98336 | tf_op jit(solution)/shard_map/ppermute | solution.py:41
  47.8 2.1 %collective-permute-done.9 = bf16[24,3072]{1,0:T(8,128)(2,1)S(1)} collective-permute-done((bf16[24,3072]{1,0:T(8,128)(2,1)S(1)}, bf16[24,3072]{1,0:T(8,128)(2,1)S(1)}, u32[]{:S(2)}, u32[]{:S(2)}) %collective-permute-start.9) | collective-permute-done | bytes 147488 | tf_op jit(solution)/shard_map/ppermute | solution.py:41
  50.0 2.9 %collective-permute-done.3 = bf16[24,3072]{1,0:T(8,128)(2,1)S(1)} collective-permute-done((bf16[24,3072]{1,0:T(8,128)(2,1)S(1)}, bf16[24,3072]{1,0:T(8,128)(2,1)S(1)}, u32[]{:S(2)}, u32[]{:S(2)}) %collective-permute-start.3) | collective-permute-done | bytes 147488 | tf_op jit(solution)/shard_map/ppermute | solution.py:41
  52.9 2.8 %collective-permute-start.10 = (bf16[48,3072]{1,0:T(8,128)(2,1)S(1)}, bf16[48,3072]{1,0:T(8,128)(2,1)S(1)}, u32[]{:S(2)}, u32[]{:S(2)}) collective-permute-start(bf16[48,3072]{1,0:T(8,128)(2,1)S(1)} %pad_maximum_fusion.3), channel_id=1, source_target_pairs={{0,6},{1,7},{2,4},{3,5},{4,2},{5,3},{6,0},{7,1},{8,14},{9,15},{10,... | collective-permute-start | bytes 884744 | tf_op jit(solution)/shard_map/ppermute | solution.py:41
  55.7 0.6 collective-permute-start.4
  56.4 4.9 %collective-permute-done.10 = bf16[48,3072]{1,0:T(8,128)(2,1)S(1)} collective-permute-done((bf16[48,3072]{1,0:T(8,128)(2,1)S(1)}, bf16[48,3072]{1,0:T(8,128)(2,1)S(1)}, u32[]{:S(2)}, u32[]{:S(2)}) %collective-permute-start.10) | collective-permute-done | bytes 294944 | tf_op jit(solution)/shard_map/ppermute | solution.py:41
  61.3 3.4 %collective-permute-done.4 = bf16[48,3072]{1,0:T(8,128)(2,1)S(1)} collective-permute-done((bf16[48,3072]{1,0:T(8,128)(2,1)S(1)}, bf16[48,3072]{1,0:T(8,128)(2,1)S(1)}, u32[]{:S(2)}, u32[]{:S(2)}) %collective-permute-start.4) | collective-permute-done | bytes 294944 | tf_op jit(solution)/shard_map/ppermute | solution.py:41
  64.7 0.5 collective-permute-start.11
  65.2 3.0 %collective-permute-start.5 = (bf16[96,3072]{1,0:T(8,128)(2,1)S(1)}, bf16[96,3072]{1,0:T(8,128)(2,1)S(1)}, u32[]{:S(2)}, u32[]{:S(2)}) collective-permute-start(bf16[96,3072]{1,0:T(8,128)(2,1)S(1)} %constant_dynamic-update-slice_fusion.refs_0_), channel_id=1, source_target_pairs={{0,6},{1,7},{2,4},{3,5},{4,2},{5,3},{6,0},{7,1},{8,14},{9,15},{10,... | collective-permute-start | bytes 1769480 | tf_op jit(solution)/shard_map/ppermute | solution.py:41
  68.2 4.5 %load.1 = (bf16[672,3072]{1,0:T(8,128)(2,1)S(1)}, bf16[672,3072]{1,0:T(8,128)(2,1)S(1)}, bf16[672,3072]{1,0:T(8,128)(2,1)S(1)}) custom-call(bf16[336,3072]{1,0:T(8,128)(2,1)S(1)} %bitcast.23, bf16[336,3072]{1,0:T(8,128)(2,1)} %collective-permute-done.17.refs_1_, bf16[336,3072]{1,0:T(8,128)(2,1)} %bitcast.5.refs_2_, ...), custom_call_target="tpu_custom_call" | custom-call | flops 12683575296 | bytes 12386304 | tf_op jit(solution)/shard_map/load/pallas_call | solution.py:73
  72.7 5.9 %experts.2.refs_6_ = bf16[64,8,3072]{2,1,0:T(8,128)(2,1)} custom-call(s32[32]{0:T(128)S(1)} %get-tuple-element.35.targets, bf16[96,3072]{1,0:T(8,128)(2,1)S(1)} %constant_dynamic-update-slice_fusion.refs_0_, bf16[96,3072]{1,0:T(8,128)(2,1)S(1)} %constant_dynamic-update-slice_fusion.5.refs_1_, ...), custom_call_target="tpu_custom_call" | custom-call | flops 3170893824 | bytes 3145728 | tf_op jit(solution)/shard_map/experts/pallas_call | solution.py:137
  78.7 6.0 %experts.3 = bf16[64,8,3072]{2,1,0:T(8,128)(2,1)} custom-call(s32[32]{0:T(128)S(1)} %get-tuple-element.36.targets, bf16[96,3072]{1,0:T(8,128)(2,1)S(1)} %collective-permute-done.5.refs_0_, bf16[96,3072]{1,0:T(8,128)(2,1)S(1)} %collective-permute-done.11.refs_1_, ...), custom_call_target="tpu_custom_call", output_to_operand_aliasing={{}: (7, {})} | custom-call | flops 3170893824 | bytes 3145728 | tf_op jit(solution)/shard_map/experts/pallas_call | solution.py:137
  84.7 5.9 %all-to-all-start = ((bf16[64,8,3072]{2,1,0:T(8,128)(2,1)}), bf16[64,8,3072]{2,1,0:T(8,128)(2,1)S(1)}, u32[]{:S(2)}, u32[]{:S(2)}) async-start(bf16[64,8,3072]{2,1,0:T(8,128)(2,1)} %experts.3), calls=%async_computation | async-start | bytes 6291456 | tf_op jit(solution)/shard_map/all_to_all | solution.py:297
  90.6 0.6 copy.44
  91.2 0.8 add_divide_fusion.1
  92.0 0.8 select_reduce_fusion.1
  92.8 2.5 %pad_maximum_fusion.1 = f32[32,48,128]{2,1,0:T(8,128)} fusion(f32[32,48,64]{2,1,0:T(8,128)} %get-tuple-element.17, f32[32,48,64]{2,1,0:T(8,128)} %subtract_add_fusion), kind=kLoop, calls=%fused_computation.5 | loop fusion | flops 196608 | bytes 1572864 | tf_op jit(solution)/shard_map/concatenate | solution.py:213
  95.3 29.1 %all-to-all-done = bf16[64,8,3072]{2,1,0:T(8,128)(2,1)S(1)} async-done(((bf16[64,8,3072]{2,1,0:T(8,128)(2,1)}), bf16[64,8,3072]{2,1,0:T(8,128)(2,1)S(1)}, u32[]{:S(2)}, u32[]{:S(2)}) %all-to-all-start) | async-done | bytes 3145760 | tf_op jit(solution)/shard_map/all_to_all | solution.py:297
  124.4 0.5 convert_reduce_fusion
  124.9 0.2 fusion
  125.2 1.4 %collective-permute-done.20 = f32[32,1536]{1,0:T(8,128)S(1)} collective-permute-done((f32[32,1536]{1,0:T(8,128)S(1)}, f32[32,1536]{1,0:T(8,128)S(1)}, u32[]{:S(2)}, u32[]{:S(2)}) %collective-permute-start.20) | collective-permute-done | bytes 196640 | tf_op jit(solution)/shard_map/ppermute | solution.py:53
  126.7 0.7 add_convert_fusion
  (83 shorter events, 2.0 us)
Async XLA Ops:
  0.6 5.5 %copy-start = (bf16[48,128,16]{1,2,0:T(8,128)(2,1)S(1)}, bf16[48,128,16]{1,2,0:T(8,128)(2,1)}, u32[]{:S(2)}) copy-start(bf16[48,128,16]{1,2,0:T(8,128)(2,1)} %param.23) | copy-start | bytes 589828
  0.6 6.3 %copy-start.6 = (f32[48,64]{1,0:T(8,128)S(1)}, f32[48,64]{1,0:T(8,128)}, u32[]{:S(2)}) copy-start(f32[48,64]{1,0:T(8,128)} %param.20) | copy-start | bytes 36868
  0.7 6.3 %copy-start.5 = (f32[48,64]{1,0:T(8,128)S(1)}, f32[48,64]{1,0:T(8,128)}, u32[]{:S(2)}) copy-start(f32[48,64]{1,0:T(8,128)} %param.21) | copy-start | bytes 36868
  1.4 5.8 %copy-start.2 = (f32[32,48,128]{2,1,0:T(8,128)S(1)}, f32[32,48,128]{2,1,0:T(8,128)}, u32[]{:S(2)}) copy-start(f32[32,48,128]{2,1,0:T(8,128)} %param.19) | copy-start | bytes 2359300
  7.2 4.3 %copy-start.4 = (bf16[48,16,128]{2,1,0:T(8,128)(2,1)S(1)}, bf16[48,16,128]{2,1,0:T(8,128)(2,1)}, u32[]{:S(2)}) copy-start(bf16[48,16,128]{2,1,0:T(8,128)(2,1)} %param.24) | copy-start | bytes 589828
  8.6 3.4 %copy-start.9 = (f32[768]{0:T(1024)S(1)}, f32[768]{0:T(1024)}, u32[]{:S(2)}) copy-start(f32[768]{0:T(1024)} %param.25) | copy-start | bytes 9220
  9.9 5.2 %copy-start.1 = (bf16[3072,336]{0,1:T(8,128)(2,1)S(1)}, bf16[3072,336]{0,1:T(8,128)(2,1)}, u32[]{:S(2)}) copy-start(bf16[3072,336]{0,1:T(8,128)(2,1)} %param.32) | copy-start | bytes 6193156
  9.9 6.3 %copy-start.8 = (s32[32,2]{0,1:T(2,128)S(1)}, s32[32,2]{0,1:T(2,128)}, u32[]{:S(2)}) copy-start(s32[32,2]{0,1:T(2,128)} %param.30) | copy-start | bytes 772
  9.9 7.3 %copy-start.10 = (s32[64]{0:T(128)S(1)}, s32[64]{0:T(128)}, u32[]{:S(2)}) copy-start(s32[64]{0:T(128)} %constant.125.clone) | copy-start | bytes 772
  10.0 7.4 %copy-start.3 = (bf16[32,3072]{1,0:T(8,128)(2,1)S(1)}, bf16[32,3072]{1,0:T(8,128)(2,1)}, u32[]{:S(2)}) copy-start(bf16[32,3072]{1,0:T(8,128)(2,1)} %param.18) | copy-start | bytes 589828
  11.5 6.1 %copy-start.7 = (f32[3072]{0:T(1024)S(1)}, f32[3072]{0:T(1024)}, u32[]{:S(2)}) copy-start(f32[3072]{0:T(1024)} %param.29) | copy-start | bytes 36868
  15.2 2.2 %collective-permute-start = (bf16[32,3072]{1,0:T(8,128)(2,1)S(1)}, bf16[32,3072]{1,0:T(8,128)(2,1)S(1)}, u32[]{:S(2)}, u32[]{:S(2)}) collective-permute-start(bf16[32,3072]{1,0:T(8,128)(2,1)S(1)} %convolution_convert_fusion.1), channel_id=1, source_target_pairs={{0,1},{1,0},{2,3},{3,2},{4,5},{5,4},{6,7},{7,6},{8,9},{9,8},{10,11... | collective-permute-start | bytes 589832 | tf_op jit(solution)/shard_map/ppermute | solution.py:53
  15.2 50.0 %collective-permute-start.17 = (bf16[336,3072]{1,0:T(8,128)(2,1)S(1)}, bf16[336,3072]{1,0:T(8,128)(2,1)}, u32[]{:S(2)}, u32[]{:S(2)}) collective-permute-start(bf16[336,3072]{1,0:T(8,128)(2,1)S(1)} %bitcast.22), channel_id=1, source_target_pairs={{0,1},{1,0},{2,3},{3,2},{4,5},{5,4},{6,7},{7,6},{8,9},{9,8},{10,11... | collective-permute-start | bytes 6193160 | tf_op jit(solution)/shard_map/ppermute | solution.py:53
  15.7 52.6 %collective-permute-start.18 = (bf16[336,3072]{1,0:T(8,128)(2,1)}, bf16[336,3072]{1,0:T(8,128)(2,1)}, u32[]{:S(2)}, u32[]{:S(2)}) collective-permute-start(bf16[336,3072]{1,0:T(8,128)(2,1)} %bitcast.5.refs_2_), channel_id=1, source_target_pairs={{0,1},{1,0},{2,3},{3,2},{4,5},{5,4},{6,7},{7,6},{8,9},{9,8},{10,11... | collective-permute-start | bytes 6193160 | tf_op jit(solution)/shard_map/ppermute | solution.py:53
  15.8 52.5 %collective-permute-start.19 = (bf16[336,3072]{1,0:T(8,128)(2,1)}, bf16[336,3072]{1,0:T(8,128)(2,1)}, u32[]{:S(2)}, u32[]{:S(2)}) collective-permute-start(bf16[336,3072]{1,0:T(8,128)(2,1)} %refs_4_.1), channel_id=1, source_target_pairs={{0,1},{1,0},{2,3},{3,2},{4,5},{5,4},{6,7},{7,6},{8,9},{9,8},{10,11... | collective-permute-start | bytes 6193160 | tf_op jit(solution)/shard_map/ppermute | solution.py:53
  17.9 6.6 %collective-permute-start.12 = (bf16[8,3072]{1,0:T(8,128)(2,1)S(1)}, bf16[8,3072]{1,0:T(8,128)(2,1)S(1)}, u32[]{:S(2)}, u32[]{:S(2)}) collective-permute-start(bf16[8,3072]{1,0:T(8,128)(2,1)S(1)} %get-tuple-element.20), channel_id=1, source_target_pairs={{0,64},{1,65},{2,66},{3,67},{4,68},{5,69},{6,70},{7,71},{8,72},{9,... | collective-permute-start | bytes 147464 | tf_op jit(solution)/shard_map/ppermute | solution.py:41
  22.1 8.1 %collective-permute-start.13 = (bf16[8,3072]{1,0:T(8,128)(2,1)S(1)}, bf16[8,3072]{1,0:T(8,128)(2,1)S(1)}, u32[]{:S(2)}, u32[]{:S(2)}) collective-permute-start(bf16[8,3072]{1,0:T(8,128)(2,1)S(1)} %get-tuple-element.18), channel_id=1, source_target_pairs={{0,88},{1,89},{2,90},{3,91},{4,92},{5,93},{6,94},{7,95},{8,80},{9,... | collective-permute-start | bytes 147464 | tf_op jit(solution)/shard_map/ppermute | solution.py:41
  24.6 7.7 %collective-permute-start.6 = (bf16[8,3072]{1,0:T(8,128)(2,1)S(1)}, bf16[8,3072]{1,0:T(8,128)(2,1)S(1)}, u32[]{:S(2)}, u32[]{:S(2)}) collective-permute-start(bf16[8,3072]{1,0:T(8,128)(2,1)S(1)} %get-tuple-element.23), channel_id=1, source_target_pairs={{0,120},{1,121},{2,122},{3,123},{4,124},{5,125},{6,126},{7,127},{8... | collective-permute-start | bytes 147464 | tf_op jit(solution)/shard_map/ppermute | solution.py:41
  30.2 4.6 %collective-permute-start.7 = (bf16[8,3072]{1,0:T(8,128)(2,1)S(1)}, bf16[8,3072]{1,0:T(8,128)(2,1)S(1)}, u32[]{:S(2)}, u32[]{:S(2)}) collective-permute-start(bf16[8,3072]{1,0:T(8,128)(2,1)S(1)} %get-tuple-element.22), channel_id=1, source_target_pairs={{0,32},{1,33},{2,34},{3,35},{4,36},{5,37},{6,38},{7,39},{8,40},{9,... | collective-permute-start | bytes 147464 | tf_op jit(solution)/shard_map/ppermute | solution.py:41
  32.3 6.5 %collective-permute-start.8 = (bf16[8,3072]{1,0:T(8,128)(2,1)S(1)}, bf16[8,3072]{1,0:T(8,128)(2,1)S(1)}, u32[]{:S(2)}, u32[]{:S(2)}) collective-permute-start(bf16[8,3072]{1,0:T(8,128)(2,1)S(1)} %get-tuple-element.21), channel_id=1, source_target_pairs={{0,56},{1,57},{2,58},{3,59},{4,60},{5,61},{6,62},{7,63},{8,48},{9,... | collective-permute-start | bytes 147464 | tf_op jit(solution)/shard_map/ppermute | solution.py:41
  34.8 7.0 %collective-permute-start.1 = (bf16[8,3072]{1,0:T(8,128)(2,1)S(1)}, bf16[8,3072]{1,0:T(8,128)(2,1)S(1)}, u32[]{:S(2)}, u32[]{:S(2)}) collective-permute-start(bf16[8,3072]{1,0:T(8,128)(2,1)S(1)} %get-tuple-element.25), channel_id=1, source_target_pairs={{0,24},{1,25},{2,26},{3,27},{4,28},{5,29},{6,30},{7,31},{8,16},{9,... | collective-permute-start | bytes 147464 | tf_op jit(solution)/shard_map/ppermute | solution.py:41
  38.7 6.0 %collective-permute-start.2 = (bf16[8,3072]{1,0:T(8,128)(2,1)S(1)}, bf16[8,3072]{1,0:T(8,128)(2,1)S(1)}, u32[]{:S(2)}, u32[]{:S(2)}) collective-permute-start(bf16[8,3072]{1,0:T(8,128)(2,1)S(1)} %get-tuple-element.24), channel_id=1, source_target_pairs={{0,96},{1,97},{2,98},{3,99},{4,100},{5,101},{6,102},{7,103},{8,104... | collective-permute-start | bytes 147464 | tf_op jit(solution)/shard_map/ppermute | solution.py:41
  41.9 5.9 %collective-permute-start.14 = (bf16[16,3072]{1,0:T(8,128)(2,1)S(1)}, bf16[16,3072]{1,0:T(8,128)(2,1)S(1)}, u32[]{:S(2)}, u32[]{:S(2)}) collective-permute-start(bf16[16,3072]{1,0:T(8,128)(2,1)S(1)} %pad_maximum_fusion.7), channel_id=1, source_target_pairs={{0,6},{1,7},{2,4},{3,5},{4,2},{5,3},{6,0},{7,1},{8,14},{9,15},{10,... | collective-permute-start | bytes 294920 | tf_op jit(solution)/shard_map/ppermute | solution.py:41
  44.7 5.2 %collective-permute-start.9 = (bf16[24,3072]{1,0:T(8,128)(2,1)S(1)}, bf16[24,3072]{1,0:T(8,128)(2,1)S(1)}, u32[]{:S(2)}, u32[]{:S(2)}) collective-permute-start(bf16[24,3072]{1,0:T(8,128)(2,1)S(1)} %pad_maximum_fusion.6), channel_id=1, source_target_pairs={{0,2},{1,3},{2,0},{3,1},{4,6},{5,7},{6,4},{7,5},{8,10},{9,11},{10,... | collective-permute-start | bytes 442376 | tf_op jit(solution)/shard_map/ppermute | solution.py:41
  47.8 5.1 %collective-permute-start.3 = (bf16[24,3072]{1,0:T(8,128)(2,1)S(1)}, bf16[24,3072]{1,0:T(8,128)(2,1)S(1)}, u32[]{:S(2)}, u32[]{:S(2)}) collective-permute-start(bf16[24,3072]{1,0:T(8,128)(2,1)S(1)} %pad_maximum_fusion.5), channel_id=1, source_target_pairs={{0,8},{1,9},{2,10},{3,11},{4,12},{5,13},{6,14},{7,15},{8,0},{9,1},... | collective-permute-start | bytes 442376 | tf_op jit(solution)/shard_map/ppermute | solution.py:41
  49.9 5.8 %collective-permute-start.15 = (bf16[32,3072]{1,0:T(8,128)(2,1)S(1)}, bf16[32,3072]{1,0:T(8,128)(2,1)S(1)}, u32[]{:S(2)}, u32[]{:S(2)}) collective-permute-start(bf16[32,3072]{1,0:T(8,128)(2,1)S(1)} %pad_maximum_fusion.4), channel_id=1, source_target_pairs={{0,8},{1,9},{2,10},{3,11},{4,12},{5,13},{6,14},{7,15},{8,0},{9,1},... | collective-permute-start | bytes 589832 | tf_op jit(solution)/shard_map/ppermute | solution.py:41
  52.9 8.3 %collective-permute-start.10 = (bf16[48,3072]{1,0:T(8,128)(2,1)S(1)}, bf16[48,3072]{1,0:T(8,128)(2,1)S(1)}, u32[]{:S(2)}, u32[]{:S(2)}) collective-permute-start(bf16[48,3072]{1,0:T(8,128)(2,1)S(1)} %pad_maximum_fusion.3), channel_id=1, source_target_pairs={{0,6},{1,7},{2,4},{3,5},{4,2},{5,3},{6,0},{7,1},{8,14},{9,15},{10,... | collective-permute-start | bytes 884744 | tf_op jit(solution)/shard_map/ppermute | solution.py:41
  55.7 9.0 %collective-permute-start.4 = (bf16[48,3072]{1,0:T(8,128)(2,1)S(1)}, bf16[48,3072]{1,0:T(8,128)(2,1)S(1)}, u32[]{:S(2)}, u32[]{:S(2)}) collective-permute-start(bf16[48,3072]{1,0:T(8,128)(2,1)S(1)} %pad_maximum_fusion.2), channel_id=1, source_target_pairs={{0,2},{1,3},{2,0},{3,1},{4,6},{5,7},{6,4},{7,5},{8,10},{9,11},{10,... | collective-permute-start | bytes 884744 | tf_op jit(solution)/shard_map/ppermute | solution.py:41
  61.3 17.4 %collective-permute-start.16 = (bf16[64,3072]{1,0:T(8,128)(2,1)S(1)}, bf16[64,3072]{1,0:T(8,128)(2,1)S(1)}, u32[]{:S(2)}, u32[]{:S(2)}) collective-permute-start(bf16[64,3072]{1,0:T(8,128)(2,1)S(1)} %constant_dynamic-update-slice_fusion.10.refs_2_), channel_id=1, source_target_pairs={{0,2},{1,3},{2,0},{3,1},{4,6},{5,7},{6,4},{7,5},{8,10},{9,11},{10,... | collective-permute-start | bytes 1179656 | tf_op jit(solution)/shard_map/ppermute | solution.py:41
  64.7 13.9 %collective-permute-start.11 = (bf16[96,3072]{1,0:T(8,128)(2,1)S(1)}, bf16[96,3072]{1,0:T(8,128)(2,1)S(1)}, u32[]{:S(2)}, u32[]{:S(2)}) collective-permute-start(bf16[96,3072]{1,0:T(8,128)(2,1)S(1)} %constant_dynamic-update-slice_fusion.5.refs_1_), channel_id=1, source_target_pairs={{0,8},{1,9},{2,10},{3,11},{4,12},{5,13},{6,14},{7,15},{8,0},{9,1},... | collective-permute-start | bytes 1769480 | tf_op jit(solution)/shard_map/ppermute | solution.py:41
  65.2 13.4 %collective-permute-start.5 = (bf16[96,3072]{1,0:T(8,128)(2,1)S(1)}, bf16[96,3072]{1,0:T(8,128)(2,1)S(1)}, u32[]{:S(2)}, u32[]{:S(2)}) collective-permute-start(bf16[96,3072]{1,0:T(8,128)(2,1)S(1)} %constant_dynamic-update-slice_fusion.refs_0_), channel_id=1, source_target_pairs={{0,6},{1,7},{2,4},{3,5},{4,2},{5,3},{6,0},{7,1},{8,14},{9,15},{10,... | collective-permute-start | bytes 1769480 | tf_op jit(solution)/shard_map/ppermute | solution.py:41
  84.7 39.8 %all-to-all-start = ((bf16[64,8,3072]{2,1,0:T(8,128)(2,1)}), bf16[64,8,3072]{2,1,0:T(8,128)(2,1)S(1)}, u32[]{:S(2)}, u32[]{:S(2)}) async-start(bf16[64,8,3072]{2,1,0:T(8,128)(2,1)} %experts.3), calls=%async_computation | async-start | bytes 6291456 | tf_op jit(solution)/shard_map/all_to_all | solution.py:297
  125.1 1.5 %collective-permute-start.20 = (f32[32,1536]{1,0:T(8,128)S(1)}, f32[32,1536]{1,0:T(8,128)S(1)}, u32[]{:S(2)}, u32[]{:S(2)}) collective-permute-start(f32[32,1536]{1,0:T(8,128)S(1)} %constant_dynamic-slice_fusion), channel_id=1, source_target_pairs={{0,1},{1,0},{2,3},{3,2},{4,5},{5,4},{6,7},{7,6},{8,9},{9,8},{10,11... | collective-permute-start | bytes 589832 | tf_op jit(solution)/shard_map/ppermute | solution.py:53

commit v2 on v1

--- a/solution.py
+++ b/solution.py
@@ -13,10 +13,10 @@
 X_SIZE = 4
 SELECT = ("za", "zb", "yb")
 SPREAD = ("ya", "xa", "xb")
-COLOURS = ((0, 3), (3, 6), (6, 8))
+COLOURS = ((0, 2), (2, 5), (5, 8))
 UNIT_CHUNK = 256
 OUT_CHUNK = 512
-COPY_GROUPS = 2
+COPY_GROUPS = 1
 
 
 def gray(value):
@@ -286,7 +286,7 @@
             across = over_links(rows, spread_links(step, colour))
             rows = jnp.concatenate([rows, across], axis=0)
         near.append(rows)
-    held_units = loaded(gates, ups, downs, ())
+    held_units = loaded(gates, ups, downs, near[-1:])
     far = []
     for colour, rows in enumerate(near):
         far.append(over_links(rows, spread_links(2, colour)))

time: 129 us -> 133 us (1.031)
  waiting for transfers between devices: 48.6 us -> 53.4 us
  other arithmetic: 11.6 us -> 9.42 us
    ppermute x16, waiting for transfers between devices: 18 us -> 24.1 us  [over_links(): return lax.ppermute(shard, ('ep', 'tp'), pairs)]
    all_to_all x1, starting transfers between devices: 5.91 us -> 9.91 us  [per_device(): lax.all_to_all(produced, 'ep', split_axis=0, concat_axis=0, tiled=True)]
    ppermute x16, starting transfers between devices: 31.9 us -> 28.3 us  [over_links(): return lax.ppermute(shard, ('ep', 'tp'), pairs)]
  transfers between devices with their start and end apart: 22 -> 22, of which waited for: 9 -> 10; matrix products, arithmetic and copies ran while one was open for 5% -> 5% of each run, Pallas kernels for 8% -> 8%
where the time goes in v2:
time: 133 us; the launch traced here: 131 us
  waiting for transfers between devices  53.4 us (40%)
  starting transfers between devices  39.4 us (30%)
  Pallas kernels  16.3 us (12%)
  other arithmetic  9.42 us (7%)
  matrix products  7.8 us (6%)
  local copies, waits for them, and re-layouts  3.79 us (3%)
    ppermute x16, starting transfers between devices, over_links(): return lax.ppermute(shard, ('ep', 'tp'), pairs)  28.3 us
    all_to_all x1, waiting for transfers between devices, per_device(): lax.all_to_all(produced, 'ep', split_axis=0, concat_axis=0, tiled=True)  27.9 us
    ppermute x16, waiting for transfers between devices, over_links(): return lax.ppermute(shard, ('ep', 'tp'), pairs)  24.1 us
    pallas_call x2, Pallas kernels, experts(): pl.pallas_call(lambda targets, *refs: expert_kernel(sizes, targets, *refs...  11.8 us
    all_to_all x1, starting transfers between devices, per_device(): lax.all_to_all(produced, 'ep', split_axis=0, concat_axis=0, tiled=True)  9.91 us
    pallas_call x1, Pallas kernels, loaded(): pl.pallas_call(lambda *refs: load_kernel(units, *refs), out_shape=[pltpu....  4.48 us
    dot_general x1, matrix products, per_device(): jnp.dot(normed, w_in, preferred_element_type=jnp.float32)  3.43 us
    dot_general x1, matrix products, per_device(): jnp.dot(activated, w_out, preferred_element_type=jnp.float32)  3.22 us
  transfers between devices with their start and end apart: 22, of which 10 were waited for; matrix products, arithmetic and copies ran while one was open for 5% of the time, Pallas kernels for 8%

profile of v2, /device:TPU:0, one launch (start us, length us, event | category | flops | bytes accessed | tf_op | source)
XLA Modules:
  0.0 131.3 jit_solution(2113801876866134414)
XLA Ops:
  0.7 0.7 exp.14
  1.4 1.1 fusion.7
  2.5 3.4 %convolution_convert_fusion.2 = bf16[32,768]{1,0:T(8,128)(2,1)S(1)} fusion(bf16[3072,768]{1,0:T(8,128)(2,1)} %param.27, bf16[32,3072]{1,0:T(8,128)(2,1)} %param.18, f32[3072]{0:T(1024)} %param.26, f32[32]{0:T(128)S(1)} %add_rsqrt_fusion.1), kind=kOutput, calls=%fused_computation.3 | convolution fusion | flops 151412736 | bytes 4976768 | tf_op jit(solution)/shard_map/dot_general | solution.py:245
  6.1 0.3 fusion.46
  6.5 0.5 copy.50
  7.0 0.2 cosine_multiply_fusion
  7.2 1.4 %fusion.43 = (bf16[32,48,64]{2,1,0:T(8,128)(2,1)S(1)}, f32[32,48,64]{2,1,0:T(8,128)}) fusion(f32[32,48,128]{2,1,0:T(8,128)S(1)} %bitcast.24, f32[48,64]{1,0:T(8,128)S(1)} %get-tuple-element.28, f32[48,64]{1,0:T(8,128)S(1)} %get-tuple-element.29, f32[32,48,128]{2,1,0:T(8,128)S(1)} %copy-done.2, f32[48,64]{1,0:T(8,128)S(1)} %get-tuple-element.27, ...), kind=kLoop, calls=%fused_computation.104 | loop fusion | flops 884736 | bytes 2211840 | tf_op jit(solution)/shard_map/neg | solution.py:209
  8.6 0.5 subtract_add_fusion
  9.1 0.8 copy-done.3
  9.9 0.2 pad_maximum_fusion
  10.2 0.3 fusion.2
  10.6 3.2 %convolution_convert_fusion.1 = bf16[32,3072]{1,0:T(8,128)(2,1)S(1)} fusion(bf16[768,3072]{1,0:T(8,128)(2,1)} %param.28, f32[32,768]{1,0:T(8,128)S(1)} %copy.40, bf16[32,768]{1,0:T(8,128)(2,1)S(1)} %convolution_convert_fusion.2, f32[768]{0:T(1024)S(1)} %copy-done.10), kind=kOutput, calls=%fused_computation.2 | convolution fusion | flops 151388160 | bytes 5065728 | tf_op jit(solution)/shard_map/dot_general | solution.py:249
  13.9 0.5 collective-permute-start.17
  14.5 0.4 collective-permute-start.19
  16.0 0.2 fusion.4
  16.3 0.3 convolution_convert_fusion
  16.6 4.6 %collective-permute-start.11 = (bf16[8,3072]{1,0:T(8,128)(2,1)S(1)}, bf16[8,3072]{1,0:T(8,128)(2,1)S(1)}, u32[]{:S(2)}, u32[]{:S(2)}) collective-permute-start(bf16[8,3072]{1,0:T(8,128)(2,1)S(1)} %get-tuple-element.20), channel_id=1, source_target_pairs={{0,56},{1,57},{2,58},{3,59},{4,60},{5,61},{6,62},{7,63},{8,48},{9,... | collective-permute-start | bytes 147464 | tf_op jit(solution)/shard_map/ppermute | solution.py:41
  21.3 3.6 %collective-permute-start.12 = (bf16[8,3072]{1,0:T(8,128)(2,1)S(1)}, bf16[8,3072]{1,0:T(8,128)(2,1)S(1)}, u32[]{:S(2)}, u32[]{:S(2)}) collective-permute-start(bf16[8,3072]{1,0:T(8,128)(2,1)S(1)} %get-tuple-element.19), channel_id=1, source_target_pairs={{0,64},{1,65},{2,66},{3,67},{4,68},{5,69},{6,70},{7,71},{8,72},{9,... | collective-permute-start | bytes 147464 | tf_op jit(solution)/shard_map/ppermute | solution.py:41
  24.8 4.5 %collective-permute-start.13 = (bf16[8,3072]{1,0:T(8,128)(2,1)S(1)}, bf16[8,3072]{1,0:T(8,128)(2,1)S(1)}, u32[]{:S(2)}, u32[]{:S(2)}) collective-permute-start(bf16[8,3072]{1,0:T(8,128)(2,1)S(1)} %get-tuple-element.18), channel_id=1, source_target_pairs={{0,88},{1,89},{2,90},{3,91},{4,92},{5,93},{6,94},{7,95},{8,80},{9,... | collective-permute-start | bytes 147464 | tf_op jit(solution)/shard_map/ppermute | solution.py:41
  29.4 0.8 collective-permute-start.5
  30.2 2.5 %collective-permute-done.13 = bf16[8,3072]{1,0:T(8,128)(2,1)S(1)} collective-permute-done((bf16[8,3072]{1,0:T(8,128)(2,1)S(1)}, bf16[8,3072]{1,0:T(8,128)(2,1)S(1)}, u32[]{:S(2)}, u32[]{:S(2)}) %collective-permute-start.13) | collective-permute-done | bytes 49184 | tf_op jit(solution)/shard_map/ppermute | solution.py:41
  32.6 1.2 collective-permute-start.1
  33.9 4.1 %collective-permute-done.1 = bf16[8,3072]{1,0:T(8,128)(2,1)S(1)} collective-permute-done((bf16[8,3072]{1,0:T(8,128)(2,1)S(1)}, bf16[8,3072]{1,0:T(8,128)(2,1)S(1)}, u32[]{:S(2)}, u32[]{:S(2)}) %collective-permute-start.1) | collective-permute-done | bytes 49184 | tf_op jit(solution)/shard_map/ppermute | solution.py:41
  37.9 4.7 %collective-permute-start.6 = (bf16[8,3072]{1,0:T(8,128)(2,1)S(1)}, bf16[8,3072]{1,0:T(8,128)(2,1)S(1)}, u32[]{:S(2)}, u32[]{:S(2)}) collective-permute-start(bf16[8,3072]{1,0:T(8,128)(2,1)S(1)} %get-tuple-element.22), channel_id=1, source_target_pairs={{0,120},{1,121},{2,122},{3,123},{4,124},{5,125},{6,126},{7,127},{8... | collective-permute-start | bytes 147464 | tf_op jit(solution)/shard_map/ppermute | solution.py:41
  42.8 2.6 %collective-permute-done.6 = bf16[8,3072]{1,0:T(8,128)(2,1)S(1)} collective-permute-done((bf16[8,3072]{1,0:T(8,128)(2,1)S(1)}, bf16[8,3072]{1,0:T(8,128)(2,1)S(1)}, u32[]{:S(2)}, u32[]{:S(2)}) %collective-permute-start.6) | collective-permute-done | bytes 49184 | tf_op jit(solution)/shard_map/ppermute | solution.py:41
  45.4 2.7 %collective-permute-start.14 = (bf16[24,3072]{1,0:T(8,128)(2,1)S(1)}, bf16[24,3072]{1,0:T(8,128)(2,1)S(1)}, u32[]{:S(2)}, u32[]{:S(2)}) collective-permute-start(bf16[24,3072]{1,0:T(8,128)(2,1)S(1)} %pad_maximum_fusion.7), channel_id=1, source_target_pairs={{0,6},{1,7},{2,4},{3,5},{4,2},{5,3},{6,0},{7,1},{8,14},{9,15},{10,... | collective-permute-start | bytes 442376 | tf_op jit(solution)/shard_map/ppermute | solution.py:41
  48.2 4.6 %collective-permute-done.2 = bf16[16,3072]{1,0:T(8,128)(2,1)S(1)} collective-permute-done((bf16[16,3072]{1,0:T(8,128)(2,1)S(1)}, bf16[16,3072]{1,0:T(8,128)(2,1)S(1)}, u32[]{:S(2)}, u32[]{:S(2)}) %collective-permute-start.2) | collective-permute-done | bytes 98336 | tf_op jit(solution)/shard_map/ppermute | solution.py:41
  52.7 0.2 collective-permute-start.8
  53.0 1.9 %collective-permute-start.3 = (bf16[32,3072]{1,0:T(8,128)(2,1)S(1)}, bf16[32,3072]{1,0:T(8,128)(2,1)S(1)}, u32[]{:S(2)}, u32[]{:S(2)}) collective-permute-start(bf16[32,3072]{1,0:T(8,128)(2,1)S(1)} %pad_maximum_fusion.5), channel_id=1, source_target_pairs={{0,2},{1,3},{2,0},{3,1},{4,6},{5,7},{6,4},{7,5},{8,10},{9,11},{10,... | collective-permute-start | bytes 589832 | tf_op jit(solution)/shard_map/ppermute | solution.py:41
  54.9 3.0 %collective-permute-done.8 = bf16[24,3072]{1,0:T(8,128)(2,1)S(1)} collective-permute-done((bf16[24,3072]{1,0:T(8,128)(2,1)S(1)}, bf16[24,3072]{1,0:T(8,128)(2,1)S(1)}, u32[]{:S(2)}, u32[]{:S(2)}) %collective-permute-start.8) | collective-permute-done | bytes 147488 | tf_op jit(solution)/shard_map/ppermute | solution.py:41
  57.9 2.1 %collective-permute-done.3 = bf16[32,3072]{1,0:T(8,128)(2,1)S(1)} collective-permute-done((bf16[32,3072]{1,0:T(8,128)(2,1)S(1)}, bf16[32,3072]{1,0:T(8,128)(2,1)S(1)}, u32[]{:S(2)}, u32[]{:S(2)}) %collective-permute-start.3) | collective-permute-done | bytes 196640 | tf_op jit(solution)/shard_map/ppermute | solution.py:41
  60.0 1.5 %collective-permute-start.9 = (bf16[48,3072]{1,0:T(8,128)(2,1)S(1)}, bf16[48,3072]{1,0:T(8,128)(2,1)S(1)}, u32[]{:S(2)}, u32[]{:S(2)}) collective-permute-start(bf16[48,3072]{1,0:T(8,128)(2,1)S(1)} %pad_maximum_fusion.3), channel_id=1, source_target_pairs={{0,6},{1,7},{2,4},{3,5},{4,2},{5,3},{6,0},{7,1},{8,14},{9,15},{10,... | collective-permute-start | bytes 884744 | tf_op jit(solution)/shard_map/ppermute | solution.py:41
  61.5 4.6 %collective-permute-done.15 = bf16[48,3072]{1,0:T(8,128)(2,1)S(1)} collective-permute-done((bf16[48,3072]{1,0:T(8,128)(2,1)S(1)}, bf16[48,3072]{1,0:T(8,128)(2,1)S(1)}, u32[]{:S(2)}, u32[]{:S(2)}) %collective-permute-start.15) | collective-permute-done | bytes 294944 | tf_op jit(solution)/shard_map/ppermute | solution.py:41
  66.1 1.7 %collective-permute-start.4 = (bf16[64,3072]{1,0:T(8,128)(2,1)S(1)}, bf16[64,3072]{1,0:T(8,128)(2,1)S(1)}, u32[]{:S(2)}, u32[]{:S(2)}) collective-permute-start(bf16[64,3072]{1,0:T(8,128)(2,1)S(1)} %pad_maximum_fusion.2.refs_0_), channel_id=1, source_target_pairs={{0,6},{1,7},{2,4},{3,5},{4,2},{5,3},{6,0},{7,1},{8,14},{9,15},{10,... | collective-permute-start | bytes 1179656 | tf_op jit(solution)/shard_map/ppermute | solution.py:41
  67.9 0.7 collective-permute-done.9
  68.7 0.8 collective-permute-start.10
  69.5 4.5 %load.1 = (bf16[672,3072]{1,0:T(8,128)(2,1)S(1)}, bf16[672,3072]{1,0:T(8,128)(2,1)S(1)}, bf16[672,3072]{1,0:T(8,128)(2,1)S(1)}) custom-call(bf16[336,3072]{1,0:T(8,128)(2,1)S(1)} %bitcast.23, bf16[336,3072]{1,0:T(8,128)(2,1)} %collective-permute-done.17.refs_1_, bf16[336,3072]{1,0:T(8,128)(2,1)} %bitcast.5.refs_2_, ...), custom_call_target="tpu_custom_call" | custom-call | flops 12683575296 | bytes 12386304 | tf_op jit(solution)/shard_map/load/pallas_call | solution.py:73
  74.0 5.9 %experts.2.refs_6_ = bf16[64,8,3072]{2,1,0:T(8,128)(2,1)} custom-call(s32[32]{0:T(128)S(1)} %get-tuple-element.34.targets, bf16[64,3072]{1,0:T(8,128)(2,1)S(1)} %pad_maximum_fusion.2.refs_0_, bf16[96,3072]{1,0:T(8,128)(2,1)S(1)} %constant_dynamic-update-slice_fusion.refs_1_, bf16[96,3072]{1,0:T(8,128)(2,1)S(1)} %constant_dynamic-update-slice_fusion.5.refs_6_.refs_2_, ...), custom_call_target="tpu_custom_call" | custom-call | flops 3170893824 | bytes 3145728 | tf_op jit(solution)/shard_map/experts/pallas_call | solution.py:137
  79.9 6.0 %experts.3 = bf16[64,8,3072]{2,1,0:T(8,128)(2,1)} custom-call(s32[32]{0:T(128)S(1)} %get-tuple-element.35.targets, bf16[64,3072]{1,0:T(8,128)(2,1)S(1)} %collective-permute-done.4.refs_0_, bf16[96,3072]{1,0:T(8,128)(2,1)S(1)} %collective-permute-done.10.refs_1_, ...), custom_call_target="tpu_custom_call", output_to_operand_aliasing={{}: (7, {})} | custom-call | flops 3170893824 | bytes 3145728 | tf_op jit(solution)/shard_map/experts/pallas_call | solution.py:137
  85.9 9.9 %all-to-all-start = ((bf16[64,8,3072]{2,1,0:T(8,128)(2,1)}), bf16[64,8,3072]{2,1,0:T(8,128)(2,1)S(1)}, u32[]{:S(2)}, u32[]{:S(2)}) async-start(bf16[64,8,3072]{2,1,0:T(8,128)(2,1)} %experts.3), calls=%async_computation | async-start | bytes 6291456 | tf_op jit(solution)/shard_map/all_to_all | solution.py:297
  95.8 0.6 copy.44
  96.4 0.8 add_divide_fusion.1
  97.2 0.8 select_reduce_fusion.1
  98.0 2.5 %pad_maximum_fusion.1 = f32[32,48,128]{2,1,0:T(8,128)} fusion(f32[32,48,64]{2,1,0:T(8,128)} %get-tuple-element.17, f32[32,48,64]{2,1,0:T(8,128)} %copy-done.3), kind=kLoop, calls=%fused_computation.5 | loop fusion | flops 196608 | bytes 1572864 | tf_op jit(solution)/shard_map/concatenate | solution.py:213
  100.5 27.9 %all-to-all-done = bf16[64,8,3072]{2,1,0:T(8,128)(2,1)S(1)} async-done(((bf16[64,8,3072]{2,1,0:T(8,128)(2,1)}), bf16[64,8,3072]{2,1,0:T(8,128)(2,1)S(1)}, u32[]{:S(2)}, u32[]{:S(2)}) %all-to-all-start) | async-done | bytes 3145760 | tf_op jit(solution)/shard_map/all_to_all | solution.py:297
  128.4 0.5 convert_reduce_fusion
  129.2 1.4 %collective-permute-done.20 = f32[32,1536]{1,0:T(8,128)S(1)} collective-permute-done((f32[32,1536]{1,0:T(8,128)S(1)}, f32[32,1536]{1,0:T(8,128)S(1)}, u32[]{:S(2)}, u32[]{:S(2)}) %collective-permute-start.20) | collective-permute-done | bytes 196640 | tf_op jit(solution)/shard_map/ppermute | solution.py:53
  130.6 0.7 add_convert_fusion
  (83 shorter events, 2.3 us)
Async XLA Ops:
  0.6 5.5 %copy-start = (bf16[48,128,16]{1,2,0:T(8,128)(2,1)S(1)}, bf16[48,128,16]{1,2,0:T(8,128)(2,1)}, u32[]{:S(2)}) copy-start(bf16[48,128,16]{1,2,0:T(8,128)(2,1)} %param.23) | copy-start | bytes 589828
  0.6 6.3 %copy-start.7 = (f32[48,64]{1,0:T(8,128)S(1)}, f32[48,64]{1,0:T(8,128)}, u32[]{:S(2)}) copy-start(f32[48,64]{1,0:T(8,128)} %param.20) | copy-start | bytes 36868
  0.7 6.3 %copy-start.6 = (f32[48,64]{1,0:T(8,128)S(1)}, f32[48,64]{1,0:T(8,128)}, u32[]{:S(2)}) copy-start(f32[48,64]{1,0:T(8,128)} %param.21) | copy-start | bytes 36868
  1.4 5.8 %copy-start.2 = (f32[32,48,128]{2,1,0:T(8,128)S(1)}, f32[32,48,128]{2,1,0:T(8,128)}, u32[]{:S(2)}) copy-start(f32[32,48,128]{2,1,0:T(8,128)} %param.19) | copy-start | bytes 2359300
  7.2 3.0 %copy-start.5 = (bf16[48,16,128]{2,1,0:T(8,128)(2,1)S(1)}, bf16[48,16,128]{2,1,0:T(8,128)(2,1)}, u32[]{:S(2)}) copy-start(bf16[48,16,128]{2,1,0:T(8,128)(2,1)} %param.24) | copy-start | bytes 589828
  8.6 2.1 %copy-start.10 = (f32[768]{0:T(1024)S(1)}, f32[768]{0:T(1024)}, u32[]{:S(2)}) copy-start(f32[768]{0:T(1024)} %param.25) | copy-start | bytes 9220
  9.1 0.9 copy-start.3
  9.1 4.8 %copy-start.1 = (bf16[3072,336]{0,1:T(8,128)(2,1)S(1)}, bf16[3072,336]{0,1:T(8,128)(2,1)}, u32[]{:S(2)}) copy-start(bf16[3072,336]{0,1:T(8,128)(2,1)} %param.32) | copy-start | bytes 6193156
  9.1 5.8 %copy-start.9 = (s32[32,2]{0,1:T(2,128)S(1)}, s32[32,2]{0,1:T(2,128)}, u32[]{:S(2)}) copy-start(s32[32,2]{0,1:T(2,128)} %param.30) | copy-start | bytes 772
  9.9 6.1 %copy-start.11 = (s32[64]{0:T(128)S(1)}, s32[64]{0:T(128)}, u32[]{:S(2)}) copy-start(s32[64]{0:T(128)} %constant.125.clone) | copy-start | bytes 772
  9.9 6.1 %copy-start.4 = (bf16[32,3072]{1,0:T(8,128)(2,1)S(1)}, bf16[32,3072]{1,0:T(8,128)(2,1)}, u32[]{:S(2)}) copy-start(bf16[32,3072]{1,0:T(8,128)(2,1)} %param.18) | copy-start | bytes 589828
  10.2 6.1 %copy-start.8 = (f32[3072]{0:T(1024)S(1)}, f32[3072]{0:T(1024)}, u32[]{:S(2)}) copy-start(f32[3072]{0:T(1024)} %param.29) | copy-start | bytes 36868
  13.9 2.2 %collective-permute-start = (bf16[32,3072]{1,0:T(8,128)(2,1)S(1)}, bf16[32,3072]{1,0:T(8,128)(2,1)S(1)}, u32[]{:S(2)}, u32[]{:S(2)}) collective-permute-start(bf16[32,3072]{1,0:T(8,128)(2,1)S(1)} %convolution_convert_fusion.1), channel_id=1, source_target_pairs={{0,1},{1,0},{2,3},{3,2},{4,5},{5,4},{6,7},{7,6},{8,9},{9,8},{10,11... | collective-permute-start | bytes 589832 | tf_op jit(solution)/shard_map/ppermute | solution.py:53
  13.9 54.8 %collective-permute-start.17 = (bf16[336,3072]{1,0:T(8,128)(2,1)S(1)}, bf16[336,3072]{1,0:T(8,128)(2,1)}, u32[]{:S(2)}, u32[]{:S(2)}) collective-permute-start(bf16[336,3072]{1,0:T(8,128)(2,1)S(1)} %bitcast.22), channel_id=1, source_target_pairs={{0,1},{1,0},{2,3},{3,2},{4,5},{5,4},{6,7},{7,6},{8,9},{9,8},{10,11... | collective-permute-start | bytes 6193160 | tf_op jit(solution)/shard_map/ppermute | solution.py:53
  14.4 55.1 %collective-permute-start.18 = (bf16[336,3072]{1,0:T(8,128)(2,1)}, bf16[336,3072]{1,0:T(8,128)(2,1)}, u32[]{:S(2)}, u32[]{:S(2)}) collective-permute-start(bf16[336,3072]{1,0:T(8,128)(2,1)} %bitcast.5.refs_2_), channel_id=1, source_target_pairs={{0,1},{1,0},{2,3},{3,2},{4,5},{5,4},{6,7},{7,6},{8,9},{9,8},{10,11... | collective-permute-start | bytes 6193160 | tf_op jit(solution)/shard_map/ppermute | solution.py:53
  14.5 55.0 %collective-permute-start.19 = (bf16[336,3072]{1,0:T(8,128)(2,1)}, bf16[336,3072]{1,0:T(8,128)(2,1)}, u32[]{:S(2)}, u32[]{:S(2)}) collective-permute-start(bf16[336,3072]{1,0:T(8,128)(2,1)} %refs_4_.1), channel_id=1, source_target_pairs={{0,1},{1,0},{2,3},{3,2},{4,5},{5,4},{6,7},{7,6},{8,9},{9,8},{10,11... | collective-permute-start | bytes 6193160 | tf_op jit(solution)/shard_map/ppermute | solution.py:53
  16.6 8.2 %collective-permute-start.11 = (bf16[8,3072]{1,0:T(8,128)(2,1)S(1)}, bf16[8,3072]{1,0:T(8,128)(2,1)S(1)}, u32[]{:S(2)}, u32[]{:S(2)}) collective-permute-start(bf16[8,3072]{1,0:T(8,128)(2,1)S(1)} %get-tuple-element.20), channel_id=1, source_target_pairs={{0,56},{1,57},{2,58},{3,59},{4,60},{5,61},{6,62},{7,63},{8,48},{9,... | collective-permute-start | bytes 147464 | tf_op jit(solution)/shard_map/ppermute | solution.py:41
  21.3 8.1 %collective-permute-start.12 = (bf16[8,3072]{1,0:T(8,128)(2,1)S(1)}, bf16[8,3072]{1,0:T(8,128)(2,1)S(1)}, u32[]{:S(2)}, u32[]{:S(2)}) collective-permute-start(bf16[8,3072]{1,0:T(8,128)(2,1)S(1)} %get-tuple-element.19), channel_id=1, source_target_pairs={{0,64},{1,65},{2,66},{3,67},{4,68},{5,69},{6,70},{7,71},{8,72},{9,... | collective-permute-start | bytes 147464 | tf_op jit(solution)/shard_map/ppermute | solution.py:41
  24.8 7.8 %collective-permute-start.13 = (bf16[8,3072]{1,0:T(8,128)(2,1)S(1)}, bf16[8,3072]{1,0:T(8,128)(2,1)S(1)}, u32[]{:S(2)}, u32[]{:S(2)}) collective-permute-start(bf16[8,3072]{1,0:T(8,128)(2,1)S(1)} %get-tuple-element.18), channel_id=1, source_target_pairs={{0,88},{1,89},{2,90},{3,91},{4,92},{5,93},{6,94},{7,95},{8,80},{9,... | collective-permute-start | bytes 147464 | tf_op jit(solution)/shard_map/ppermute | solution.py:41
  29.4 13.3 %collective-permute-start.5 = (bf16[8,3072]{1,0:T(8,128)(2,1)S(1)}, bf16[8,3072]{1,0:T(8,128)(2,1)S(1)}, u32[]{:S(2)}, u32[]{:S(2)}) collective-permute-start(bf16[8,3072]{1,0:T(8,128)(2,1)S(1)} %get-tuple-element.23), channel_id=1, source_target_pairs={{0,96},{1,97},{2,98},{3,99},{4,100},{5,101},{6,102},{7,103},{8,104... | collective-permute-start | bytes 147464 | tf_op jit(solution)/shard_map/ppermute | solution.py:41
  32.6 5.3 %collective-permute-start.1 = (bf16[8,3072]{1,0:T(8,128)(2,1)S(1)}, bf16[8,3072]{1,0:T(8,128)(2,1)S(1)}, u32[]{:S(2)}, u32[]{:S(2)}) collective-permute-start(bf16[8,3072]{1,0:T(8,128)(2,1)S(1)} %get-tuple-element.24), channel_id=1, source_target_pairs={{0,24},{1,25},{2,26},{3,27},{4,28},{5,29},{6,30},{7,31},{8,16},{9,... | collective-permute-start | bytes 147464 | tf_op jit(solution)/shard_map/ppermute | solution.py:41
  37.9 7.4 %collective-permute-start.6 = (bf16[8,3072]{1,0:T(8,128)(2,1)S(1)}, bf16[8,3072]{1,0:T(8,128)(2,1)S(1)}, u32[]{:S(2)}, u32[]{:S(2)}) collective-permute-start(bf16[8,3072]{1,0:T(8,128)(2,1)S(1)} %get-tuple-element.22), channel_id=1, source_target_pairs={{0,120},{1,121},{2,122},{3,123},{4,124},{5,125},{6,126},{7,127},{8... | collective-permute-start | bytes 147464 | tf_op jit(solution)/shard_map/ppermute | solution.py:41
  42.7 5.4 %collective-permute-start.7 = (bf16[8,3072]{1,0:T(8,128)(2,1)S(1)}, bf16[8,3072]{1,0:T(8,128)(2,1)S(1)}, u32[]{:S(2)}, u32[]{:S(2)}) collective-permute-start(bf16[8,3072]{1,0:T(8,128)(2,1)S(1)} %get-tuple-element.21), channel_id=1, source_target_pairs={{0,32},{1,33},{2,34},{3,35},{4,36},{5,37},{6,38},{7,39},{8,40},{9,... | collective-permute-start | bytes 147464 | tf_op jit(solution)/shard_map/ppermute | solution.py:41
  45.4 7.6 %collective-permute-start.14 = (bf16[24,3072]{1,0:T(8,128)(2,1)S(1)}, bf16[24,3072]{1,0:T(8,128)(2,1)S(1)}, u32[]{:S(2)}, u32[]{:S(2)}) collective-permute-start(bf16[24,3072]{1,0:T(8,128)(2,1)S(1)} %pad_maximum_fusion.7), channel_id=1, source_target_pairs={{0,6},{1,7},{2,4},{3,5},{4,2},{5,3},{6,0},{7,1},{8,14},{9,15},{10,... | collective-permute-start | bytes 442376 | tf_op jit(solution)/shard_map/ppermute | solution.py:41
  48.1 4.6 %collective-permute-start.2 = (bf16[16,3072]{1,0:T(8,128)(2,1)S(1)}, bf16[16,3072]{1,0:T(8,128)(2,1)S(1)}, u32[]{:S(2)}, u32[]{:S(2)}) collective-permute-start(bf16[16,3072]{1,0:T(8,128)(2,1)S(1)} %pad_maximum_fusion.8), channel_id=1, source_target_pairs={{0,8},{1,9},{2,10},{3,11},{4,12},{5,13},{6,14},{7,15},{8,0},{9,1},... | collective-permute-start | bytes 294920 | tf_op jit(solution)/shard_map/ppermute | solution.py:41
  52.7 5.1 %collective-permute-start.8 = (bf16[24,3072]{1,0:T(8,128)(2,1)S(1)}, bf16[24,3072]{1,0:T(8,128)(2,1)S(1)}, u32[]{:S(2)}, u32[]{:S(2)}) collective-permute-start(bf16[24,3072]{1,0:T(8,128)(2,1)S(1)} %pad_maximum_fusion.6), channel_id=1, source_target_pairs={{0,2},{1,3},{2,0},{3,1},{4,6},{5,7},{6,4},{7,5},{8,10},{9,11},{10,... | collective-permute-start | bytes 442376 | tf_op jit(solution)/shard_map/ppermute | solution.py:41
  53.0 7.0 %collective-permute-start.3 = (bf16[32,3072]{1,0:T(8,128)(2,1)S(1)}, bf16[32,3072]{1,0:T(8,128)(2,1)S(1)}, u32[]{:S(2)}, u32[]{:S(2)}) collective-permute-start(bf16[32,3072]{1,0:T(8,128)(2,1)S(1)} %pad_maximum_fusion.5), channel_id=1, source_target_pairs={{0,2},{1,3},{2,0},{3,1},{4,6},{5,7},{6,4},{7,5},{8,10},{9,11},{10,... | collective-permute-start | bytes 589832 | tf_op jit(solution)/shard_map/ppermute | solution.py:41
  57.9 8.3 %collective-permute-start.15 = (bf16[48,3072]{1,0:T(8,128)(2,1)S(1)}, bf16[48,3072]{1,0:T(8,128)(2,1)S(1)}, u32[]{:S(2)}, u32[]{:S(2)}) collective-permute-start(bf16[48,3072]{1,0:T(8,128)(2,1)S(1)} %pad_maximum_fusion.4), channel_id=1, source_target_pairs={{0,8},{1,9},{2,10},{3,11},{4,12},{5,13},{6,14},{7,15},{8,0},{9,1},... | collective-permute-start | bytes 884744 | tf_op jit(solution)/shard_map/ppermute | solution.py:41
  60.0 8.6 %collective-permute-start.9 = (bf16[48,3072]{1,0:T(8,128)(2,1)S(1)}, bf16[48,3072]{1,0:T(8,128)(2,1)S(1)}, u32[]{:S(2)}, u32[]{:S(2)}) collective-permute-start(bf16[48,3072]{1,0:T(8,128)(2,1)S(1)} %pad_maximum_fusion.3), channel_id=1, source_target_pairs={{0,6},{1,7},{2,4},{3,5},{4,2},{5,3},{6,0},{7,1},{8,14},{9,15},{10,... | collective-permute-start | bytes 884744 | tf_op jit(solution)/shard_map/ppermute | solution.py:41
  66.1 13.8 %collective-permute-start.4 = (bf16[64,3072]{1,0:T(8,128)(2,1)S(1)}, bf16[64,3072]{1,0:T(8,128)(2,1)S(1)}, u32[]{:S(2)}, u32[]{:S(2)}) collective-permute-start(bf16[64,3072]{1,0:T(8,128)(2,1)S(1)} %pad_maximum_fusion.2.refs_0_), channel_id=1, source_target_pairs={{0,6},{1,7},{2,4},{3,5},{4,2},{5,3},{6,0},{7,1},{8,14},{9,15},{10,... | collective-permute-start | bytes 1179656 | tf_op jit(solution)/shard_map/ppermute | solution.py:41
  68.6 11.3 %collective-permute-start.16 = (bf16[96,3072]{1,0:T(8,128)(2,1)S(1)}, bf16[96,3072]{1,0:T(8,128)(2,1)S(1)}, u32[]{:S(2)}, u32[]{:S(2)}) collective-permute-start(bf16[96,3072]{1,0:T(8,128)(2,1)S(1)} %constant_dynamic-update-slice_fusion.5.refs_6_.refs_2_), channel_id=1, source_target_pairs={{0,2},{1,3},{2,0},{3,1},{4,6},{5,7},{6,4},{7,5},{8,10},{9,11},{10,... | collective-permute-start | bytes 1769480 | tf_op jit(solution)/shard_map/ppermute | solution.py:41
  68.7 11.3 %collective-permute-start.10 = (bf16[96,3072]{1,0:T(8,128)(2,1)S(1)}, bf16[96,3072]{1,0:T(8,128)(2,1)S(1)}, u32[]{:S(2)}, u32[]{:S(2)}) collective-permute-start(bf16[96,3072]{1,0:T(8,128)(2,1)S(1)} %constant_dynamic-update-slice_fusion.refs_1_), channel_id=1, source_target_pairs={{0,8},{1,9},{2,10},{3,11},{4,12},{5,13},{6,14},{7,15},{8,0},{9,1},... | collective-permute-start | bytes 1769480 | tf_op jit(solution)/shard_map/ppermute | solution.py:41
  85.9 42.5 %all-to-all-start = ((bf16[64,8,3072]{2,1,0:T(8,128)(2,1)}), bf16[64,8,3072]{2,1,0:T(8,128)(2,1)S(1)}, u32[]{:S(2)}, u32[]{:S(2)}) async-start(bf16[64,8,3072]{2,1,0:T(8,128)(2,1)} %experts.3), calls=%async_computation | async-start | bytes 6291456 | tf_op jit(solution)/shard_map/all_to_all | solution.py:297
  129.1 1.5 %collective-permute-start.20 = (f32[32,1536]{1,0:T(8,128)S(1)}, f32[32,1536]{1,0:T(8,128)S(1)}, u32[]{:S(2)}, u32[]{:S(2)}) collective-permute-start(f32[32,1536]{1,0:T(8,128)S(1)} %constant_dynamic-slice_fusion), channel_id=1, source_target_pairs={{0,1},{1,0},{2,3},{3,2},{4,5},{5,4},{6,7},{7,6},{8,9},{9,8},{10,11... | collective-permute-start | bytes 589832 | tf_op jit(solution)/shard_map/ppermute | solution.py:53
